TPU v7x, 32 devices: a whole 2x2x4 slice. The times are simulated.
32 devices in a mesh: ep: 32 (over z, y, x, core).
Axes of the slice: x: 2, y: 2, z: 4, core: 2. Of those that a mesh axis runs over, the one named last changes fastest.
Arguments:
- tokens: bfloat16 [384, 2048], P('ep'), may hold values from -6 to 6
- cache_latent: bfloat16 [384, 1024, 512], P('ep'), may hold values from -180 to 180
- cache_rope: bfloat16 [384, 1024, 64], P('ep'), may hold values from -6 to 6
- cache_lengths: int32 [384], P('ep'), may hold values from 1 to 1024, as said below
- expert_ids: int32 [384, 6], P('ep'), may hold values from 0 to 15, as said below
- route_weight: float32 [384, 6], P('ep'), may hold values from 1 to 2
- attn_gain: float32 [2048], replicated, may hold values from 0.1 to 1.9
- q_gain: float32 [512], replicated, may hold values from 0.1 to 1.9
- kv_gain: float32 [512], replicated, may hold values from 0.1 to 1.9
- moe_gain: float32 [2048], replicated, may hold values from 0.1 to 1.9
- w_qdown: bfloat16 [2048, 512], replicated, may hold values from -0.125 to 0.125
- w_kvdown: bfloat16 [2048, 512], replicated, may hold values from -0.125 to 0.125
- w_krope: bfloat16 [2048, 64], replicated, may hold values from -0.125 to 0.125
- w_qup: bfloat16 [512, 1536], replicated, may hold values from -0.25 to 0.25
- w_kup: bfloat16 [512, 1024], replicated, may hold values from -0.5 to 0.5
- w_vup: bfloat16 [512, 1024], replicated, may hold values from -0.25 to 0.25
- w_out: bfloat16 [1024, 2048], replicated, may hold values from -0.1875 to 0.1875
- expert_gate: bfloat16 [32, 2048, 256], P('ep'), may hold values from -0.125 to 0.125
- expert_up: bfloat16 [32, 2048, 256], P('ep'), may hold values from -0.125 to 0.125
- expert_down: bfloat16 [32, 256, 2048], P('ep'), may hold values from -0.25 to 0.25
Outputs:
- mixed: float32 [384, 2048], P('ep')
- new_latent: bfloat16 [384, 512], P('ep')
- new_rope_key: bfloat16 [384, 64], P('ep')
Inputs may be any that keep to these rules, and one draw needn't show every extreme that they name: `cache_lengths`: some sequence holds 1024 positions. `expert_ids`: each row names 6 different experts of one group g, numbered g * 16 to g * 16 + 15; among the rows of one device no expert is named more than 5 times, and some expert exactly 5 times.
All inputs are finite; a program needn't handle non-finite values.
Results may differ from a plain program's by a relative error of at most 0.03.
Values may be sent and summed in bfloat16 or wider, within the bound.
No kernel may reach another device: no remote copies, remote signals or barrier semaphores. Data moves between devices by JAX's collectives and lax.ppermute only.
A program may use at most 128 MiB of HBM per device.

v0:
```python
import jax
import jax.numpy as jnp
from jax import lax
from jax.sharding import PartitionSpec as P

HEADS = 8
KV_RANK = 512
NOPE_DIM = 128
ROPE_DIM = 64
VALUE_DIM = 128
GROUP_SIZE = 16
TOP_K = 6
BLOCK_POS = 512
SEQ_DEV = 12


EPS = 1e-06
THETA = 10000.0


def partner(value, axis, bit):
    mask = 2**bit
    pairs = [(source, source ^ mask) for source in range(lax.axis_size(axis))]
    return lax.ppermute(value, axis, pairs)


def norm_gain(values, gain_vec):
    values = values.astype(jnp.float32)
    return values * lax.rsqrt(jnp.mean(values * values, axis=-1, keepdims=True) + EPS) * gain_vec


def rotary_angles(lengths):
    half_width = ROPE_DIM // 2
    inverse = THETA ** (-jnp.arange(half_width, dtype=jnp.float32) / half_width)
    return lengths.astype(jnp.float32)[:, None] * inverse[None, :]


def rotate(values, angles):
    half_width = values.shape[-1] // 2
    first_half = values[..., :half_width]
    second = values[..., half_width:]
    cosine = jnp.cos(angles)
    sine_part = jnp.sin(angles)
    return jnp.concatenate(
        [first_half * cosine - second * sine_part, second * cosine + first_half * sine_part],
        axis=-1,
    )


def attend(
    tokens,
    cache_latent,
    cache_rope,
    cache_lengths,
    attn_gain,
    q_gain,
    kv_gain,
    w_qdown,
    w_kvdown,
    w_krope,
    w_qup,
    w_kup,
    w_vup,
    w_out,
):
    row_count = tokens.shape[0]
    score_scale = (NOPE_DIM + ROPE_DIM) ** (-0.5)
    normed = norm_gain(tokens, attn_gain).astype(jnp.bfloat16)
    q_low = norm_gain(jnp.dot(normed, w_qdown, preferred_element_type=jnp.float32), q_gain).astype(
        jnp.bfloat16
    )
    query_all = jnp.dot(q_low, w_qup, preferred_element_type=jnp.float32).reshape(
        row_count, HEADS, NOPE_DIM + ROPE_DIM
    )
    angles = rotary_angles(cache_lengths)
    q_nope = query_all[:, :, :NOPE_DIM].astype(jnp.bfloat16)
    q_rope = rotate(query_all[:, :, NOPE_DIM:], angles[:, None, :]).astype(jnp.bfloat16)
    new_latent = norm_gain(
        jnp.dot(normed, w_kvdown, preferred_element_type=jnp.float32), kv_gain
    ).astype(jnp.bfloat16)
    new_rope_key = rotate(
        jnp.dot(normed, w_krope, preferred_element_type=jnp.float32), angles
    ).astype(jnp.bfloat16)
    q_latent = jnp.einsum(
        "thn,chn->thc",
        q_nope,
        w_kup.reshape(KV_RANK, HEADS, NOPE_DIM),
        preferred_element_type=jnp.float32,
    ).astype(jnp.bfloat16)
    own_score = (
        jnp.einsum("thc,tc->th", q_latent, new_latent, preferred_element_type=jnp.float32)
        + jnp.einsum("thr,tr->th", q_rope, new_rope_key, preferred_element_type=jnp.float32)
    ) * score_scale
    run_sum = jnp.broadcast_to(
        new_latent.astype(jnp.float32)[:, None, :], (row_count, HEADS, KV_RANK)
    )
    run_total = jnp.ones((row_count, HEADS), jnp.float32)
    block_total = (jnp.max(cache_lengths) + BLOCK_POS - 1) // BLOCK_POS

    def block_step(block_index, carry):
        run_peak, run_total, run_sum = carry
        block_start = block_index * BLOCK_POS
        latent_block = lax.dynamic_slice_in_dim(cache_latent, block_start, BLOCK_POS, 1)
        rope_block = lax.dynamic_slice_in_dim(cache_rope, block_start, BLOCK_POS, 1)
        scores = (
            jnp.einsum("thc,tpc->thp", q_latent, latent_block, preferred_element_type=jnp.float32)
            + jnp.einsum("thr,tpr->thp", q_rope, rope_block, preferred_element_type=jnp.float32)
        ) * score_scale
        valid_mask = (block_start + jnp.arange(BLOCK_POS, dtype=jnp.int32))[
            None, None, :
        ] < cache_lengths[:, None, None]
        scores = jnp.where(valid_mask, scores, -jnp.inf)
        new_peak = jnp.maximum(run_peak, jnp.max(scores, axis=2))
        shrink = jnp.exp(run_peak - new_peak)
        block_probs = jnp.exp(scores - new_peak[:, :, None])
        run_total = run_total * shrink + jnp.sum(block_probs, axis=2)
        run_sum = run_sum * shrink[:, :, None] + jnp.einsum(
            "thp,tpc->thc",
            block_probs.astype(jnp.bfloat16),
            latent_block,
            preferred_element_type=jnp.float32,
        )
        return (new_peak, run_total, run_sum)

    run_peak, run_total, run_sum = lax.fori_loop(
        0, block_total, block_step, (own_score, run_total, run_sum)
    )
    o_latent = (run_sum / run_total[:, :, None]).astype(jnp.bfloat16)
    heads_out = (
        jnp.einsum(
            "thc,chv->thv",
            o_latent,
            w_vup.reshape(KV_RANK, HEADS, VALUE_DIM),
            preferred_element_type=jnp.float32,
        )
        .astype(jnp.bfloat16)
        .reshape(row_count, HEADS * VALUE_DIM)
    )
    mixed_attn = (
        tokens.astype(jnp.float32) + jnp.dot(heads_out, w_out, preferred_element_type=jnp.float32)
    ).astype(jnp.bfloat16)
    return (mixed_attn, new_latent, new_rope_key)


def capacity_of(half_count):
    group_count = half_count // 2 // GROUP_SIZE
    group_most = min(SEQ_DEV, max(3, 2 * ((SEQ_DEV + group_count - 1) // group_count)))
    return (TOP_K * group_most + GROUP_SIZE - 1) // GROUP_SIZE


def mix_experts(moe_in, expert_ids, route_weight, expert_gate, expert_up, expert_down):
    row_count, model_width = moe_in.shape
    top_count = expert_ids.shape[1]
    half_count = lax.axis_size("ep")
    slot_count = capacity_of(half_count)
    per_core = (slot_count + 1) // 2
    gate_half = expert_gate[0]
    up_half = expert_up[0]
    down_half = expert_down[0]
    flat_ids = expert_ids.reshape(-1)
    one_hot = (flat_ids[:, None] == jnp.arange(half_count // 2, dtype=jnp.int32)[None, :]).astype(
        jnp.int32
    )
    earlier = jnp.cumsum(one_hot, axis=0) - one_hot
    slot_rank = jnp.sum(earlier * one_hot, axis=1)
    owner_ids = jnp.arange(half_count, dtype=jnp.int32) // 2
    parity_ids = jnp.arange(half_count, dtype=jnp.int32) % 2
    wanted_rank = (
        2 * jnp.arange(per_core, dtype=jnp.int32)[None, None, :] + parity_ids[None, :, None]
    )
    placed = (flat_ids[:, None, None] == owner_ids[None, :, None]) & (
        slot_rank[:, None, None] == wanted_rank
    )
    placed = placed.reshape(row_count * top_count, half_count * per_core).astype(jnp.float32)
    chosen = jnp.max(placed.reshape(row_count, top_count, half_count * per_core), axis=1).astype(
        jnp.bfloat16
    )
    outgoing = jnp.einsum("sx,sd->xd", chosen, moe_in, preferred_element_type=jnp.float32).astype(
        jnp.bfloat16
    )
    own_rows = lax.all_to_all(
        outgoing.reshape(half_count, per_core, model_width),
        "ep",
        split_axis=0,
        concat_axis=0,
        tiled=True,
    )
    sibling = partner(own_rows, "ep", 0)
    slot_rows = jnp.concatenate([own_rows, sibling], axis=1)
    flat_rows = slot_rows.reshape(-1, model_width)
    hidden = (
        jax.nn.silu(jnp.dot(flat_rows, gate_half, preferred_element_type=jnp.float32))
        * jnp.dot(flat_rows, up_half, preferred_element_type=jnp.float32)
    ).astype(jnp.bfloat16)
    outputs = (
        jnp.dot(hidden, down_half, preferred_element_type=jnp.float32)
        .astype(jnp.bfloat16)
        .reshape(slot_rows.shape)
    )
    from_sibling = partner(outputs[:, per_core:], "ep", 0)
    pair_sum = outputs[:, :per_core].astype(jnp.float32) + from_sibling.astype(jnp.float32)
    returned = lax.all_to_all(pair_sum, "ep", split_axis=0, concat_axis=0, tiled=True)
    per_route = jnp.dot(
        placed,
        returned.reshape(half_count * per_core, model_width),
        precision=lax.Precision.HIGHEST,
        preferred_element_type=jnp.float32,
    )
    per_route = per_route.reshape(row_count, top_count, model_width)
    return jnp.sum(route_weight[:, :, None] * per_route, axis=1)


def shards(
    tokens,
    cache_latent,
    cache_rope,
    cache_lengths,
    expert_ids,
    route_weight,
    attn_gain,
    q_gain,
    kv_gain,
    moe_gain,
    w_qdown,
    w_kvdown,
    w_krope,
    w_qup,
    w_kup,
    w_vup,
    w_out,
    expert_gate,
    expert_up,
    expert_down,
):
    mixer_weights = (
        attn_gain,
        q_gain,
        kv_gain,
        w_qdown,
        w_kvdown,
        w_krope,
        w_qup,
        w_kup,
        w_vup,
        w_out,
    )
    mixed_attn, new_latent, new_rope_key = attend(
        tokens, cache_latent, cache_rope, cache_lengths, *mixer_weights
    )
    moe_in = norm_gain(mixed_attn, moe_gain).astype(jnp.bfloat16)
    moe_out = mix_experts(moe_in, expert_ids, route_weight, expert_gate, expert_up, expert_down)
    mixed = mixed_attn.astype(jnp.float32) + moe_out
    return (mixed, new_latent, new_rope_key)


def solution(mesh):
    placed = (
        P("ep", None),
        P("ep", None, None),
        P("ep", None, None),
        P("ep"),
        P("ep", None),
        P("ep", None),
        P(),
        P(),
        P(),
        P(),
        P(),
        P(),
        P(),
        P(),
        P(),
        P(),
        P(),
        P("ep", None, None),
        P("ep", None, None),
        P("ep", None, None),
    )
    return jax.shard_map(
        shards,
        mesh=mesh,
        in_specs=placed,
        out_specs=(P("ep", None), P("ep", None), P("ep", None)),
        check_vma=False,
    )
```

profile of v0, /device:TPU:0, one launch (start us, length us, event | category | flops | bytes accessed | tf_op | source)
XLA Modules:
  0.0 106.8 jit_solution(619388758719337516)
XLA Ops:
  0.7 1.5 %fusion.63 = (s32[]{:T(128)}, f32[12]{0:T(128)S(1)}) fusion(s32[12]{0:T(128)} %param.25), kind=kLoop, calls=%fused_computation.104 | loop fusion | flops 23 | bytes 100 | tf_op jit(solution)/shard_map/reduce_max | solution.py:98
  2.8 0.5 multiply_power_fusion
  3.3 1.0 fusion.33
  4.3 1.4 %multiply_reduce_fusion.1 = (f32[12]{0:T(128)S(1)}, f32[12,512]{1,0:T(8,128)S(1)}) fusion(bf16[2048,512]{1,0:T(8,128)(2,1)S(1)} %copy-done, bf16[12,2048]{1,0:T(8,128)(2,1)} %param.22, f32[2048]{0:T(1024)} %param.28, f32[12]{0:T(128)S(1)} %add_rsqrt_fusion.3), kind=kOutput, calls=%fused_computation.67 | convolution fusion | flops 25276404 | bytes 2179168 | tf_op jit(solution)/shard_map/dot_general | solution.py:79
  5.9 0.6 and_select_fusion.1
  6.5 2.3 %multiply_reduce_fusion.2 = (f32[12]{0:T(128)S(1)}, f32[12,512]{1,0:T(8,128)S(1)}) fusion(bf16[2048,512]{1,0:T(8,128)(2,1)} %param.32, bf16[12,2048]{1,0:T(8,128)(2,1)S(1)} %copy-done.3, f32[2048]{0:T(1024)S(1)} %copy-done.6, f32[12]{0:T(128)S(1)} %add_rsqrt_fusion.3), kind=kOutput, calls=%fused_computation.69 | convolution fusion | flops 25276404 | bytes 2179168 | tf_op jit(solution)/shard_map/dot_general | solution.py:69
  8.8 0.4 fusion.49
  9.2 0.1 reshape.305
  9.3 1.2 %fusion.56 = f32[12,64]{1,0:T(8,128)S(1)} fusion(bf16[2048,64]{0,1:T(8,128)(2,1)} %param.34, bf16[12,2048]{1,0:T(8,128)(2,1)S(1)} %copy-done.3, f32[2048]{0:T(1024)S(1)} %copy-done.6, f32[12]{0:T(128)S(1)} %add_rsqrt_fusion.3), kind=kOutput, calls=%fused_computation.100 | convolution fusion | flops 3244032 | bytes 322608 | tf_op jit(solution)/shard_map/dot_general | solution.py:82
  10.5 0.4 fusion.21
  10.9 0.1 copy.50
  11.0 0.8 subtract_convert_fusion.1
  11.7 0.1 subtract_convert_fusion
  11.8 0.1 pad_maximum_fusion.1
  11.9 0.1 fusion.79
  12.0 0.1 fusion.53
  12.1 0.1 fusion.46
  12.3 18.1 %while.14 = (s32[]{:T(128)}, f32[12,8]{1,0:T(8,128)S(1)}, f32[12,8]{1,0:T(8,128)S(1)}, f32[12,8,512]{2,1,0:T(8,128)S(1)}, s32[]{:T(128)}, /*index=5*/s32[12]{0:T...) while((s32[]{:T(128)}, f32[12,8]{1,0:T(8,128)S(1)}, ...), condition=%wide.region_7.8_spmd, body=%wide.region_4.7_spmd.sunk | while | flops 107453120 | bytes 21184784 | solution.py:125
  12.4 4.6 %fusion.96 = f32[12,512,8]{1,2,0:T(8,128)S(1)} fusion(bf16[12,8,512]{2,1,0:T(8,128)(2,1)S(1)} %get-tuple-element.242, bf16[12,1024,512]{2,1,0:T(8,128)(2,1)} %get-tuple-element.241, s32[]{:T(128)S(6)} %select_n.46), kind=kOutput, calls=%fused_computation.2.clone.1 | convolution fusion | flops 50331648 | bytes 6586372 | tf_op jit(solution)/shard_map/while/body/thc,tpc->thp/dot_general | solution.py:106
  17.0 0.1 broadcast_compare_fusion.3
  17.1 0.3 fusion.97
  17.4 0.2 fusion.98
  17.6 3.7 %fusion.99 = f32[12,8,512]{2,1,0:T(8,128)S(1)} fusion(bf16[12,1024,512]{2,1,0:T(8,128)(2,1)} %get-tuple-element.241, s32[]{:T(128)S(6)} %select_n.46, f32[12,8,512]{2,1,0:T(8,128)S(1)} %get-tuple-element.224, f32[12,8,512]{2,1,0:T(8,128)S(1)} %get-tuple-element.204, f32[12,8]{1,0:T(8,128)S(1)} %get-tuple-element.206, f32[12,8]{1,0:T(8,128)S(1)} %max.4), kind=kOutput, calls=%fused_computation.6.clone.1 | convolution fusion | flops 50528256 | bytes 6882052 | tf_op jit(solution)/shard_map/while/body/thp,tpc->thc/dot_general | solution.py:117
  21.4 4.6 %fusion.96 = f32[12,512,8]{1,2,0:T(8,128)S(1)} fusion(bf16[12,8,512]{2,1,0:T(8,128)(2,1)S(1)} %get-tuple-element.242, bf16[12,1024,512]{2,1,0:T(8,128)(2,1)} %get-tuple-element.241, s32[]{:T(128)S(6)} %select_n.46), kind=kOutput, calls=%fused_computation.2.clone.1 | convolution fusion | flops 50331648 | bytes 6586372 | tf_op jit(solution)/shard_map/while/body/thc,tpc->thp/dot_general | solution.py:106
  26.0 0.1 broadcast_compare_fusion.3
  26.1 0.3 fusion.97
  26.4 0.2 fusion.98
  26.6 3.7 %fusion.99 = f32[12,8,512]{2,1,0:T(8,128)S(1)} fusion(bf16[12,1024,512]{2,1,0:T(8,128)(2,1)} %get-tuple-element.241, s32[]{:T(128)S(6)} %select_n.46, f32[12,8,512]{2,1,0:T(8,128)S(1)} %get-tuple-element.224, f32[12,8,512]{2,1,0:T(8,128)S(1)} %get-tuple-element.204, f32[12,8]{1,0:T(8,128)S(1)} %get-tuple-element.206, f32[12,8]{1,0:T(8,128)S(1)} %max.4), kind=kOutput, calls=%fused_computation.6.clone.1 | convolution fusion | flops 50528256 | bytes 6882052 | tf_op jit(solution)/shard_map/while/body/thp,tpc->thc/dot_general | solution.py:117
  30.4 0.1 divide_convert_fusion
  30.5 1.5 %fusion.22 = bf16[12,8,128]{2,0,1:T(8,128)(2,1)S(1)} fusion(bf16[12,8,512]{2,1,0:T(8,128)(2,1)S(1)} %divide_convert_fusion, bf16[512,1024]{1,0:T(8,128)(2,1)} %param.37), kind=kOutput, calls=%fused_computation.31 | convolution fusion | flops 12595200 | bytes 1171456 | tf_op jit(solution)/shard_map/thc,chv->thv/dot_general | solution.py:130
  32.1 3.0 %multiply_reduce_fusion = (f32[12]{0:T(128)S(1)}, f32[12,2048]{1,0:T(8,128)S(1)}) fusion(bf16[12,1024]{1,0:T(8,128)(2,1)S(1)} %bitcast.70, bf16[1024,2048]{1,0:T(8,128)(2,1)} %param.38, bf16[12,2048]{1,0:T(8,128)(2,1)S(1)} %copy-done.3), kind=kOutput, calls=%fused_computation.54 | convolution fusion | flops 50479092 | bytes 4366384 | tf_op jit(solution)/shard_map/dot_general | solution.py:140
  35.1 0.1 copy.55
  35.2 0.1 eq.66
  35.3 0.1 fusion.44
  35.4 0.1 reduce_window_sum.11
  35.5 0.2 select_reduce_fusion
  35.7 0.1 eq.76
  35.7 0.1 broadcast_compare_fusion.1
  35.9 0.4 and.62
  36.3 0.1 add.143
  36.4 0.1 add.145
  36.6 0.4 convert_reduce_fusion
  37.0 0.3 convolution_convert_fusion.1
  37.3 0.2 reshape.309
  37.5 21.2 %all_to_all.10 = bf16[32,3,2048]{2,1,0:T(4,128)(2,1)S(1)} all-to-all(bf16[32,3,2048]{2,1,0:T(4,128)(2,1)S(1)} %reshape.309), channel_id=1, replica_groups=mesh['ep'=32] {'ep'}, dimensions={0} | all-to-all | bytes 786432 | tf_op jit(solution)/shard_map/all_to_all | solution.py:181
  58.7 1.9 %collective-permute-done = bf16[32,3,2048]{2,1,0:T(4,128)(2,1)S(1)} collective-permute-done((bf16[32,3,2048]{2,1,0:T(4,128)(2,1)S(1)}, bf16[32,3,2048]{2,1,0:T(4,128)(2,1)S(1)}, u32[]{:S(2)}, u32[]{:S(2)}) %collective-permute-start) | collective-permute-done | bytes 393248 | tf_op jit(solution)/shard_map/ppermute | solution.py:24
  60.6 1.5 %pad_maximum_fusion = bf16[32,6,2048]{2,1,0:T(8,128)(2,1)} fusion(bf16[32,3,2048]{2,1,0:T(4,128)(2,1)S(1)} %collective-permute-done, bf16[32,3,2048]{2,1,0:T(4,128)(2,1)S(1)} %all_to_all.10), kind=kLoop, calls=%fused_computation.36 | loop fusion | flops 1572864 | bytes 1572864 | tf_op jit(solution)/shard_map/concatenate | solution.py:189
  62.1 1.4 %reshape.310 = bf16[192,2048]{1,0:T(8,128)(2,1)S(1)} reshape(bf16[32,6,2048]{2,1,0:T(8,128)(2,1)} %pad_maximum_fusion) | data formatting | bytes 1572864 | tf_op jit(solution)/shard_map/reshape | solution.py:190
  63.5 1.6 %fusion.28 = f32[192,256]{1,0:T(8,128)S(1)} fusion(bf16[192,2048]{1,0:T(8,128)(2,1)S(1)} %reshape.310, bf16[1,2048,256]{2,1,0:T(8,128)(2,1)} %param.40), kind=kOutput, calls=%fused_computation.38 | convolution fusion | flops 201326592 | bytes 2031616 | tf_op jit(solution)/shard_map/dot_general | solution.py:193
  65.1 3.5 %convolution_convert_fusion = bf16[192,2048]{1,0:T(8,128)(2,1)} fusion(bf16[1,256,2048]{2,1,0:T(8,128)(2,1)} %param.41, f32[192,256]{1,0:T(8,128)S(1)} %fusion.28, bf16[192,2048]{1,0:T(8,128)(2,1)S(1)} %reshape.310, bf16[1,2048,256]{2,1,0:T(8,128)(2,1)} %param.39), kind=kOutput, calls=%fused_computation.21 | convolution fusion | flops 403341312 | bytes 3866624 | tf_op jit(solution)/shard_map/dot_general | solution.py:196
  68.6 1.3 %reshape.311 = bf16[32,6,2048]{2,1,0:T(8,128)(2,1)S(1)} reshape(bf16[192,2048]{1,0:T(8,128)(2,1)} %convolution_convert_fusion) | data formatting | bytes 1572864 | tf_op jit(solution)/shard_map/reshape | solution.py:198
  70.0 0.3 slice.38
  70.3 0.2 collective-permute-start.1
  70.5 1.8 %collective-permute-done.1 = bf16[32,3,2048]{2,1,0:T(4,128)(2,1)S(1)} collective-permute-done((bf16[32,3,2048]{2,1,0:T(4,128)(2,1)S(1)}, bf16[32,3,2048]{2,1,0:T(4,128)(2,1)S(1)}, u32[]{:S(2)}, u32[]{:S(2)}) %collective-permute-start.1) | collective-permute-done | bytes 393248 | tf_op jit(solution)/shard_map/ppermute | solution.py:24
  72.3 1.3 %convert_add_fusion = f32[32,3,2048]{2,1,0:T(4,128)} fusion(bf16[32,3,2048]{2,1,0:T(4,128)(2,1)S(1)} %collective-permute-done.1, bf16[32,6,2048]{2,1,0:T(8,128)(2,1)S(1)} %reshape.311), kind=kLoop, calls=%fused_computation.42 | loop fusion | flops 589824 | bytes 1572864 | tf_op jit(solution)/shard_map/add | solution.py:201
  73.6 3.0 %all-to-all-start.1 = ((f32[32,3,2048]{2,1,0:T(4,128)}), f32[32,3,2048]{2,1,0:T(4,128)S(1)}, u32[]{:S(2)}, u32[]{:S(2)}) async-start(f32[32,3,2048]{2,1,0:T(4,128)} %convert_add_fusion), calls=%async_computation.1 | async-start | bytes 2097152 | tf_op jit(solution)/shard_map/all_to_all | solution.py:202
  76.7 0.1 compare_and_fusion
  76.8 0.4 and.61
  77.2 0.1 copy.54
  77.3 0.7 pad_maximum_fusion.2
  77.9 24.8 %all-to-all-done.1 = f32[32,3,2048]{2,1,0:T(4,128)S(1)} async-done(((f32[32,3,2048]{2,1,0:T(4,128)}), f32[32,3,2048]{2,1,0:T(4,128)S(1)}, u32[]{:S(2)}, u32[]{:S(2)}) %all-to-all-start.1) | async-done | bytes 786464 | tf_op jit(solution)/shard_map/all_to_all | solution.py:202
  102.8 1.3 %reshape.317 = f32[96,2048,1]{1,0,2:T(8,128)} reshape(f32[32,3,2048]{2,1,0:T(4,128)S(1)} %all-to-all-done.1) | data formatting | bytes 1572864 | tf_op jit(solution)/shard_map/reshape | solution.py:205
  104.1 2.1 %fusion.20 = f32[12,2048]{1,0:T(8,128)S(1)} fusion(f32[96,2048,1]{1,0,2:T(8,128)} %reshape.317, pred[12,6,96]{1,0,2:T(8,128)(4,1)S(1)} %and.61, f32[12,6]{1,0:T(8,128)S(1)} %copy.54), kind=kOutput, calls=%fused_computation.27 | convolution fusion | flops 170139648 | bytes 891936 | tf_op jit(solution)/shard_map/dot_general | solution.py:203
  106.1 0.7 add.150
  (59 shorter events, 0.6 us)
Async XLA Ops:
  0.6 3.7 %copy-start = (bf16[2048,512]{1,0:T(8,128)(2,1)S(1)}, bf16[2048,512]{1,0:T(8,128)(2,1)}, u32[]{:S(2)}) copy-start(bf16[2048,512]{1,0:T(8,128)(2,1)} %param.33) | copy-start | bytes 6291460
  0.6 5.8 %copy-start.3 = (bf16[12,2048]{1,0:T(8,128)(2,1)S(1)}, bf16[12,2048]{1,0:T(8,128)(2,1)}, u32[]{:S(2)}) copy-start(bf16[12,2048]{1,0:T(8,128)(2,1)} %param.22) | copy-start | bytes 147460
  0.7 5.8 %copy-start.6 = (f32[2048]{0:T(1024)S(1)}, f32[2048]{0:T(1024)}, u32[]{:S(2)}) copy-start(f32[2048]{0:T(1024)} %param.28) | copy-start | bytes 24580
  0.7 5.0 %copy-start.9 = (f32[512]{0:T(512)S(1)}, f32[512]{0:T(512)}, u32[]{:S(2)}) copy-start(f32[512]{0:T(512)} %param.30) | copy-start | bytes 6148
  4.3 4.5 %copy-start.12 = (f32[512]{0:T(512)S(1)}, f32[512]{0:T(512)}, u32[]{:S(2)}) copy-start(f32[512]{0:T(512)} %param.29) | copy-start | bytes 6148
  5.9 6.4 %copy-start.5 = (bf16[12,512]{1,0:T(8,128)(2,1)}, bf16[12,512]{1,0:T(8,128)(2,1)S(1)}, u32[]{:S(2)}) copy-start(bf16[12,512]{1,0:T(8,128)(2,1)S(1)} %multiply_convert_fusion.4) | copy-start | bytes 36868
  6.5 2.3 %copy-start.2 = (bf16[512,1536]{1,0:T(8,128)(2,1)S(1)}, bf16[512,1536]{1,0:T(8,128)(2,1)}, u32[]{:S(2)}) copy-start(bf16[512,1536]{1,0:T(8,128)(2,1)} %param.35) | copy-start | bytes 4718596
  6.5 4.0 %copy-start.4 = (bf16[512,1024]{1,0:T(8,128)(2,1)S(1)}, bf16[512,1024]{1,0:T(8,128)(2,1)}, u32[]{:S(2)}) copy-start(bf16[512,1024]{1,0:T(8,128)(2,1)} %param.36) | copy-start | bytes 3145732
  8.8 3.5 %copy-start.7 = (s32[12]{0:T(128)S(1)}, s32[12]{0:T(128)}, u32[]{:S(2)}) copy-start(s32[12]{0:T(128)} %param.25) | copy-start | bytes 148
  12.4 4.7 %copy-start.1 = (bf16[12,1024,64]{1,2,0:T(8,128)(2,1)S(1)}, bf16[12,1024,64]{1,2,0:T(8,128)(2,1)}, u32[]{:S(2)}) copy-start(bf16[12,1024,64]{1,2,0:T(8,128)(2,1)} %get-tuple-element.243) | copy-start | bytes 4718596 | tf_op jit(solution)/shard_map/while
  21.4 4.7 %copy-start.1 = (bf16[12,1024,64]{1,2,0:T(8,128)(2,1)S(1)}, bf16[12,1024,64]{1,2,0:T(8,128)(2,1)}, u32[]{:S(2)}) copy-start(bf16[12,1024,64]{1,2,0:T(8,128)(2,1)} %get-tuple-element.243) | copy-start | bytes 4718596 | tf_op jit(solution)/shard_map/while
  32.1 3.0 %copy-start.10 = (s32[12,6]{0,1:T(8,128)S(1)}, s32[12,6]{0,1:T(8,128)}, u32[]{:S(2)}) copy-start(s32[12,6]{0,1:T(8,128)} %param.26) | copy-start | bytes 868
  32.1 3.6 %copy-start.13 = (s32[32]{0:T(128)S(1)}, s32[32]{0:T(128)}, u32[]{:S(2)}) copy-start(s32[32]{0:T(128)} %and_select_fusion.1) | copy-start | bytes 388
  32.1 4.9 %copy-start.8 = (f32[2048]{0:T(1024)S(1)}, f32[2048]{0:T(1024)}, u32[]{:S(2)}) copy-start(f32[2048]{0:T(1024)} %param.31) | copy-start | bytes 24580
  58.7 1.9 %collective-permute-start = (bf16[32,3,2048]{2,1,0:T(4,128)(2,1)S(1)}, bf16[32,3,2048]{2,1,0:T(4,128)(2,1)S(1)}, u32[]{:S(2)}, u32[]{:S(2)}) collective-permute-start(bf16[32,3,2048]{2,1,0:T(4,128)(2,1)S(1)} %all_to_all.10), channel_id=1, source_target_pairs={{0,1},{1,0},{2,3},{3,2},{4,5},{5,4},{6,7},{7,6},{8,9},{9,8},{10,11... | collective-permute-start | bytes 1179656 | tf_op jit(solution)/shard_map/ppermute | solution.py:24
  70.3 6.9 %copy-start.11 = (f32[12,6]{0,1:T(8,128)S(1)}, f32[12,6]{0,1:T(8,128)}, u32[]{:S(2)}) copy-start(f32[12,6]{0,1:T(8,128)} %param.27) | copy-start | bytes 868
  70.3 2.0 %collective-permute-start.1 = (bf16[32,3,2048]{2,1,0:T(4,128)(2,1)S(1)}, bf16[32,3,2048]{2,1,0:T(4,128)(2,1)S(1)}, u32[]{:S(2)}, u32[]{:S(2)}) collective-permute-start(bf16[32,3,2048]{2,1,0:T(4,128)(2,1)S(1)} %slice.38), channel_id=1, source_target_pairs={{0,1},{1,0},{2,3},{3,2},{4,5},{5,4},{6,7},{7,6},{8,9},{9,8},{10,11... | collective-permute-start | bytes 1179656 | tf_op jit(solution)/shard_map/ppermute | solution.py:24
  73.6 29.2 %all-to-all-start.1 = ((f32[32,3,2048]{2,1,0:T(4,128)}), f32[32,3,2048]{2,1,0:T(4,128)S(1)}, u32[]{:S(2)}, u32[]{:S(2)}) async-start(f32[32,3,2048]{2,1,0:T(4,128)} %convert_add_fusion), calls=%async_computation.1 | async-start | bytes 2097152 | tf_op jit(solution)/shard_map/all_to_all | solution.py:202
where the time goes:
time: 108 us; the launch traced here: 107 us
  matrix products  35.1 us (32%)
  waiting for transfers between devices  28.5 us (26%)
  blocking collectives  21.2 us (20%)
  other arithmetic  10.6 us (10%)
  local copies, waits for them, and re-layouts  6.36 us (6%)
  starting transfers between devices  3.18 us (3%)
  between operations  1.73 us (2%)
    all_to_all x1, waiting for transfers between devices, mix_experts(): lax.all_to_all(pair_sum, 'ep', split_axis=0, concat_axis=0, tiled=True)  24.8 us
    all_to_all x1, blocking collectives, mix_experts(): lax.all_to_all(outgoing.reshape(half_count, per_core, model_width), 'ep',...  21.2 us
    dot_general x2, matrix products, block_step(): jnp.einsum('thc,tpc->thp', q_latent, latent_block, preferred_element_type...  9.26 us
    dot_general x2, matrix products, block_step(): jnp.einsum('thp,tpc->thc', block_probs.astype(jnp.bfloat16), latent_block...  7.5 us
    ppermute x2, waiting for transfers between devices, partner(): return lax.ppermute(value, axis, pairs)  3.68 us
    dot_general x1, matrix products, mix_experts(): jnp.dot(hidden, down_half, preferred_element_type=jnp.float32)  3.47 us
    all_to_all x1, starting transfers between devices, mix_experts(): lax.all_to_all(pair_sum, 'ep', split_axis=0, concat_axis=0, tiled=True)  2.97 us
    dot_general x1, matrix products, attend(): jnp.dot(heads_out, w_out, preferred_element_type=jnp.float32)  2.96 us
  transfers between devices with their start and end apart: 3, of which 3 were waited for; matrix products, arithmetic and copies ran while one was open for 1% of the time, Pallas kernels for 0%

commit v1 on v0

v1 whole, which is shorter than its diff:
```python
import jax
import jax.numpy as jnp
import numpy as np
from jax import lax
from jax.experimental import pallas as pl
from jax.experimental.pallas import tpu as pltpu
from jax.sharding import PartitionSpec as P

HEADS = 8
NOPE_DIM = 128
ROPE_DIM = 64
VALUE_DIM = 128
GROUP_SIZE = 16
TOP_K = 6
SEQ_DEV = 12
LANES = 128
ROWS = 16
SEQ_STEP = 4
SEQ_AHEAD = 8

EPS = 1e-06
THETA = 10000.0
F32 = jnp.float32
BF16 = jnp.bfloat16


def mm(a, b):
    return jnp.dot(a, b, preferred_element_type=F32)


def mm_t(a, b):
    return lax.dot_general(a, b, (((1,), (1,)), ((), ())), preferred_element_type=F32)


def partner(value, axis, bit):
    mask = 2**bit
    pairs = [(source, source ^ mask) for source in range(lax.axis_size(axis))]
    return lax.ppermute(value, axis, pairs)


def norm_gain(values, gain_vec):
    return values * lax.rsqrt(jnp.mean(values * values, axis=-1, keepdims=True) + EPS) * gain_vec


def capacity_of(half_count):
    group_count = half_count // 2 // GROUP_SIZE
    group_most = min(SEQ_DEV, max(3, 2 * ((SEQ_DEV + group_count - 1) // group_count)))
    return (TOP_K * group_most + GROUP_SIZE - 1) // GROUP_SIZE


def inverse_row():
    half_width = ROPE_DIM // 2
    inverse = THETA ** (-np.arange(half_width) / half_width)
    return np.tile(inverse, LANES // half_width).reshape(1, LANES).astype(np.float32)


def mixer(n_seq, n_pos, width, lat, expert_count, slot_count):
    scale = (NOPE_DIM + ROPE_DIM) ** (-0.5)
    half = width // 2
    chunks = half // LANES

    def body(
        len_hbm,
        tokens_hbm,
        inverse_hbm,
        ids_hbm,
        weight_hbm,
        attn_gain_hbm,
        q_gain_hbm,
        kv_gain_hbm,
        moe_gain_hbm,
        qdown_hbm,
        kvdown_hbm,
        krope_hbm,
        qup_hbm,
        kup_hbm,
        vup_hbm,
        out_hbm,
        latent_hbm,
        rope_hbm,
        gate_hbm,
        up_hbm,
        down_hbm,
        mixed_hbm,
        new_latent_ref,
        new_rope_ref,
        send_ref,
        combine_hbm,
        gate_ref,
        up_ref,
        down_ref,
        len_ref,
        tokens_ref,
        inverse_ref,
        ids_ref,
        weight_ref,
        attn_gain_ref,
        q_gain_ref,
        kv_gain_ref,
        moe_gain_ref,
        mixed_ref,
        combine_ref,
        qdown,
        kvdown,
        krope,
        qup,
        kup,
        vup,
        w_out,
        latent,
        rope,
        q_lat_s,
        q_rope_s,
        o_lat_s,
        rows_s,
        latent_row_s,
        key_row_s,
        w_sem,
        c_sem,
        r_sem,
        s_sem,
        o_sem,
    ):
        small = [
            pltpu.make_async_copy(source, target, s_sem.at[i])
            for i, (source, target) in enumerate(
                (
                    (tokens_hbm, tokens_ref),
                    (attn_gain_hbm, attn_gain_ref),
                    (len_hbm, len_ref),
                    (inverse_hbm, inverse_ref),
                    (ids_hbm, ids_ref),
                    (weight_hbm, weight_ref),
                    (q_gain_hbm, q_gain_ref),
                    (kv_gain_hbm, kv_gain_ref),
                    (moe_gain_hbm, moe_gain_ref),
                )
            )
        ]
        for copy in small:
            copy.start()

        def weight_copy(i):
            pairs = [
                (qdown_hbm, qdown),
                (kvdown_hbm, kvdown),
                (krope_hbm, krope),
                (qup_hbm, qup),
                (kup_hbm, kup),
                (vup_hbm, vup),
                (out_hbm, w_out),
                (gate_hbm, gate_ref),
                (up_hbm, up_ref),
                (down_hbm, down_ref),
            ]
            return pltpu.make_async_copy(pairs[i][0], pairs[i][1], w_sem.at[i])

        def latent_copy(t):
            return pltpu.make_async_copy(latent_hbm.at[t], latent.at[t], c_sem.at[t])

        def rope_copy(t):
            return pltpu.make_async_copy(rope_hbm.at[t], rope.at[t], r_sem.at[t])

        def cache_start(t):
            latent_copy(t).start()
            rope_copy(t).start()

        weight_copy(0).start()
        weight_copy(1).start()

        expert_row = lax.broadcasted_iota(jnp.int32, (expert_count, LANES), 0)
        for copy in small:
            copy.wait()
        token_lane = lax.broadcasted_iota(jnp.int32, (n_seq, LANES), 1)
        token_row = lax.broadcasted_iota(jnp.int32, (n_seq, LANES), 0)
        spread = (token_lane % ROWS == token_row).astype(BF16)
        valid = lax.broadcasted_iota(jnp.int32, (TOP_K, LANES), 1) % ROWS < n_seq
        ids = jnp.where(valid, mm(ids_ref[...].astype(F32).astype(BF16), spread), -1.0)
        ids = ids.astype(jnp.int32)
        weight = weight_ref[...]
        weight_high = weight.astype(BF16)
        weight_low = mm((weight - weight_high.astype(F32)).astype(BF16), spread)
        weight_high = mm(weight_high, spread)
        taken = jnp.zeros((expert_count, LANES), F32)
        share_high = jnp.zeros((expert_count, LANES), F32)
        share_low = jnp.zeros((expert_count, LANES), F32)
        for k in range(TOP_K):
            hit = ids[k : k + 1, :] == expert_row
            taken = jnp.where(hit, 1.0, taken)
            share_high = jnp.where(hit, weight_high[k : k + 1, :], share_high)
            share_low = jnp.where(hit, weight_low[k : k + 1, :], share_low)
        for i in range(2, 5):
            weight_copy(i).start()
        row_a = lax.broadcasted_iota(jnp.int32, (LANES, LANES), 0)
        row_b = lax.broadcasted_iota(jnp.int32, (LANES, LANES), 1)
        before = ((row_a // ROWS == row_b // ROWS) & (row_a < row_b)).astype(BF16)
        rank = mm(taken.astype(BF16), before)
        rank = jnp.where(taken > 0.5, rank, -1.0)
        rows_per = slot_count * chunks
        shape3 = (expert_count, rows_per, LANES)
        sub = lax.broadcasted_iota(jnp.int32, shape3, 1)
        lane3 = lax.broadcasted_iota(jnp.int32, shape3, 2)
        placed = (rank[:, None, :] == (sub // chunks).astype(F32)) & (sub % chunks == lane3 // ROWS)
        flat = (expert_count * rows_per, LANES)
        picked = jnp.where(placed, 1.0, 0.0).reshape(flat).astype(BF16)
        for part, share in ((0, share_high), (1, share_low)):
            back = jnp.where(placed, jnp.broadcast_to(share[:, None, :], shape3), 0.0)
            combine_ref[part] = back.reshape(flat).T.astype(BF16)
        combine_copy = pltpu.make_async_copy(combine_ref, combine_hbm, o_sem.at[0])
        combine_copy.start()
        rows_s[...] = jnp.zeros_like(rows_s)

        tokens = tokens_ref[...].astype(F32)
        normed = norm_gain(tokens, attn_gain_ref[...]).astype(BF16)
        weight_copy(0).wait()
        cache_start(0)
        cache_start(1)
        q_low = norm_gain(mm(normed, qdown[...]), q_gain_ref[...]).astype(BF16)
        weight_copy(1).wait()
        cache_start(2)
        cache_start(3)
        new_latent = norm_gain(mm(normed, kvdown[...]), kv_gain_ref[...]).astype(BF16)
        new_latent_ref[...] = new_latent
        latent_row_s[...] = new_latent.astype(F32)
        weight_copy(2).wait()
        key_raw = mm_t(normed, krope[...])
        low_half = lax.broadcasted_iota(jnp.int32, (n_seq, LANES), 1)
        first_quarter = low_half % ROPE_DIM < ROPE_DIM // 2
        low_half = low_half < ROPE_DIM

        length = jnp.zeros((n_seq, LANES), F32)
        for t in range(n_seq):
            length = jnp.where(token_row == t, len_ref[t].astype(F32), length)
        angle = length * inverse_ref[...]
        cosine = jnp.cos(angle)
        sine = jnp.sin(angle)
        sine = jnp.where(first_quarter, -sine, sine)

        def rotate(v):
            swapped = jnp.where(
                first_quarter,
                pltpu.roll(v, LANES - ROPE_DIM // 2, 1),
                pltpu.roll(v, ROPE_DIM // 2, 1),
            )
            return v * cosine + swapped * sine

        new_key = rotate(jnp.concatenate([key_raw, key_raw], axis=1))
        new_key = new_key.astype(BF16)
        new_rope_ref[...] = new_key[:, :ROPE_DIM]
        key_row_s[...] = jnp.where(low_half, new_key.astype(F32), 0.0)

        weight_copy(3).wait()
        for t in range(4, SEQ_AHEAD):
            cache_start(t)
        query = mm(q_low, qup[...])
        weight_copy(4).wait()
        for pair in range(HEADS // 2):
            base = 3 * LANES * pair
            first = query[:, base : base + LANES]
            middle = query[:, base + LANES : base + 2 * LANES]
            last = query[:, base + 2 * LANES : base + 3 * LANES]
            second = jnp.where(
                low_half, pltpu.roll(middle, ROPE_DIM, 1), pltpu.roll(last, ROPE_DIM, 1)
            )
            both = rotate(jnp.where(low_half, middle, last))
            for side, nope in ((0, first), (1, second)):
                head = 2 * pair + side
                q_lat_s[:, head, :] = mm_t(
                    nope.astype(BF16), kup[:, head * NOPE_DIM : (head + 1) * NOPE_DIM]
                )
                turned = both if side == 0 else pltpu.roll(both, ROPE_DIM, 1)
                q_rope_s[:, head, :] = turned

        position = lax.broadcasted_iota(jnp.int32, (HEADS, n_pos), 1)

        def step(group, carry):
            start = group * SEQ_STEP
            for j in range(SEQ_STEP):

                @pl.when(start + j + SEQ_AHEAD < n_seq)
                def _(ahead=start + j + SEQ_AHEAD):
                    cache_start(ahead)

            @pl.when((start + SEQ_AHEAD >= n_seq) & (start + SEQ_AHEAD < n_seq + SEQ_STEP))
            def _():
                for i in range(5, 10):
                    weight_copy(i).start()

            for j in range(SEQ_STEP):
                latent_copy(start + j).wait()
                rope_copy(start + j).wait()
            for j in range(SEQ_STEP):
                t = start + j
                q_lat = q_lat_s[t].astype(BF16)
                q_rope = q_rope_s[t].astype(BF16)
                own_row = latent_row_s[pl.ds(t, 1), :]
                own_key = key_row_s[pl.ds(t, 1), :]
                own = (
                    jnp.sum(q_lat.astype(F32) * own_row, axis=1, keepdims=True)
                    + jnp.sum(q_rope.astype(F32) * own_key, axis=1, keepdims=True)
                ) * scale
                scores = (
                    mm_t(q_lat, latent[t]) + mm(q_rope[:, :ROPE_DIM], rope[t])
                ) * scale
                scores = jnp.where(position < len_ref[t], scores, -jnp.inf)
                peak = jnp.maximum(jnp.max(scores, axis=1, keepdims=True), own)
                probs = jnp.exp(scores - peak)
                own_prob = jnp.exp(own - peak)
                total = jnp.sum(probs, axis=1, keepdims=True) + own_prob
                summed = mm(probs.astype(BF16), latent[t]) + own_prob.astype(BF16).astype(F32) * own_row
                o_lat_s[:, pl.ds(t, 1), :] = (summed / total)[:, None, :]
            return carry

        lax.fori_loop(0, n_seq // SEQ_STEP, step, 0)

        weight_copy(5).wait()
        parts = []
        for head in range(HEADS):
            parts.append(
                mm(
                    o_lat_s[head].astype(BF16),
                    vup[:, head * VALUE_DIM : (head + 1) * VALUE_DIM],
                ).astype(BF16)
            )
        heads_out = jnp.concatenate(parts, axis=1)
        weight_copy(6).wait()
        for i in range(7, 10):
            weight_copy(i).wait()
        mixed = (tokens + mm(heads_out, w_out[...])).astype(BF16).astype(F32)
        mixed_ref[...] = mixed
        mixed_copy = pltpu.make_async_copy(mixed_ref, mixed_hbm, o_sem.at[1])
        mixed_copy.start()
        moe_in = norm_gain(mixed, moe_gain_ref[...])
        for side in range(2):
            for r in range(chunks):
                col = side * half + r * LANES
                rows_s[side, r * ROWS : r * ROWS + n_seq, :] = moe_in[:, col : col + LANES]
            out = mm(picked, rows_s[side].astype(BF16)).astype(BF16)
            send_ref[:, side] = out.reshape(shape3)
        combine_copy.wait()
        mixed_copy.wait()

    return body


def run_mixer(tokens, cache_latent, cache_rope, cache_lengths, ids, weights, gains, mats, experts, half_count):
    n_seq, width = tokens.shape
    _, n_pos, lat = cache_latent.shape
    expert_count = half_count // 2
    slot_count = capacity_of(half_count)
    chunks = width // 2 // LANES
    rows_per = slot_count * chunks
    vmem = pl.BlockSpec(memory_space=pltpu.VMEM)
    hbm = pl.BlockSpec(memory_space=pltpu.HBM)
    small = [
        cache_lengths,
        tokens,
        jnp.asarray(inverse_row()),
        ids.T,
        weights.T,
        *[g.reshape(1, -1) for g in gains],
    ]
    return pl.pallas_call(
        mixer(n_seq, n_pos, width, lat, expert_count, slot_count),
        out_shape=(
            pltpu.HBM((n_seq, width), F32),
            jax.ShapeDtypeStruct((n_seq, lat), BF16),
            jax.ShapeDtypeStruct((n_seq, ROPE_DIM), BF16),
            jax.ShapeDtypeStruct((expert_count, 2, rows_per, LANES), BF16),
            pltpu.HBM((2, LANES, expert_count * rows_per), BF16),
            *[jax.ShapeDtypeStruct(m.shape, BF16) for m in experts],
        ),
        in_specs=[hbm] * (len(small) + len(mats) + 2 + len(experts)),
        out_specs=(hbm, vmem, vmem, vmem, hbm) + (vmem,) * len(experts),
        scratch_shapes=[pltpu.SMEM((n_seq,), jnp.int32)]
        + [pltpu.VMEM(m.shape, m.dtype) for m in small[1:]]
        + [
            pltpu.VMEM((n_seq, width), F32),
            pltpu.VMEM((2, LANES, expert_count * rows_per), BF16),
        ]
        + [pltpu.VMEM(m.shape, BF16) for m in mats]
        + [
            pltpu.VMEM((n_seq, n_pos, lat), BF16),
            pltpu.VMEM((n_seq, ROPE_DIM, n_pos), BF16),
            pltpu.VMEM((n_seq, HEADS, lat), F32),
            pltpu.VMEM((n_seq, HEADS, LANES), F32),
            pltpu.VMEM((HEADS, n_seq, lat), F32),
            pltpu.VMEM((2, chunks * ROWS, LANES), F32),
            pltpu.VMEM((n_seq, lat), F32),
            pltpu.VMEM((n_seq, LANES), F32),
            pltpu.SemaphoreType.DMA((len(mats) + len(experts),)),
            pltpu.SemaphoreType.DMA((n_seq,)),
            pltpu.SemaphoreType.DMA((n_seq,)),
            pltpu.SemaphoreType.DMA((len(small),)),
            pltpu.SemaphoreType.DMA((2,)),
        ],
        compiler_params=pltpu.CompilerParams(vmem_limit_bytes=44 * 1024 * 1024),
        name="mixer",
    )(
        *[
            pltpu.with_memory_space_constraint(m, pltpu.HBM)
            for m in (*small, *mats, cache_latent, jnp.swapaxes(cache_rope, 1, 2), *experts)
        ],
    )


def expert_kernel(rows, chunks):
    half = chunks * LANES

    def body(side_ref, own_ref, other_ref, gate_ref, up_ref, down_ref, keep_ref, pass_ref, wide):
        side = side_ref[0]
        halves = []
        for slot, ref in ((0, own_ref), (1, other_ref)):
            wide[slot] = ref[...].astype(F32)
            cols = [wide[slot, pl.ds(r, rows, stride=chunks), :].astype(BF16) for r in range(chunks)]
            halves.append(jnp.concatenate(cols, axis=1))
        here = pl.ds(pl.multiple_of(side * half, half), half)
        there = pl.ds(pl.multiple_of((1 - side) * half, half), half)
        gate = mm(halves[0], gate_ref[here, :]) + mm(halves[1], gate_ref[there, :])
        up = mm(halves[0], up_ref[here, :]) + mm(halves[1], up_ref[there, :])
        hidden = (gate * jax.nn.sigmoid(gate) * up).astype(BF16)
        for slot, cols, ref in ((0, there, pass_ref), (1, here, keep_ref)):
            out = mm(hidden, down_ref[:, cols])
            for r in range(chunks):
                wide[slot, pl.ds(r, rows, stride=chunks), :] = out[:, r * LANES : (r + 1) * LANES]
            ref[...] = wide[slot].astype(BF16)

    return body


def run_expert(side, own, other, gate, up, down):
    count, _ = own.shape
    chunks = gate.shape[0] // 2 // LANES
    vmem = pl.BlockSpec(memory_space=pltpu.VMEM)
    return pl.pallas_call(
        expert_kernel(count // chunks, chunks),
        out_shape=(jax.ShapeDtypeStruct(own.shape, BF16),) * 2,
        in_specs=[pl.BlockSpec(memory_space=pltpu.SMEM)] + [vmem] * 5,
        out_specs=(vmem, vmem),
        scratch_shapes=[pltpu.VMEM((2, count, LANES), F32)],
        compiler_params=pltpu.CompilerParams(vmem_limit_bytes=40 * 1024 * 1024),
        name="expert_half",
    )(side, own, other, gate, up, down)


def combine_kernel(n_seq, chunks):
    half = chunks * LANES

    def body(mixed_ref, combine_ref, rows_ref, out_ref):
        expert_count, _, rows_per, _ = rows_ref.shape
        for side in range(2):
            rows = rows_ref[:, side].reshape(expert_count * rows_per, LANES)
            total = mm(combine_ref[0], rows) + mm(combine_ref[1], rows)
            for r in range(chunks):
                col = slice(side * half + r * LANES, side * half + (r + 1) * LANES)
                out_ref[:, col] = mixed_ref[:, col] + total[r * ROWS : r * ROWS + n_seq, :]

    return body


def run_combine(mixed, combine, rows):
    n_seq, width = mixed.shape
    vmem = pl.BlockSpec(memory_space=pltpu.VMEM)
    return pl.pallas_call(
        combine_kernel(n_seq, width // 2 // LANES),
        out_shape=jax.ShapeDtypeStruct(mixed.shape, F32),
        in_specs=[vmem] * 3,
        out_specs=vmem,
        compiler_params=pltpu.CompilerParams(vmem_limit_bytes=40 * 1024 * 1024),
        name="combine",
    )(mixed, combine, rows)


def shards(
    tokens,
    cache_latent,
    cache_rope,
    cache_lengths,
    expert_ids,
    route_weight,
    attn_gain,
    q_gain,
    kv_gain,
    moe_gain,
    w_qdown,
    w_kvdown,
    w_krope,
    w_qup,
    w_kup,
    w_vup,
    w_out,
    expert_gate,
    expert_up,
    expert_down,
):
    half_count = lax.axis_size("ep")
    mixed_attn, new_latent, new_rope_key, send, combine, *experts = run_mixer(
        tokens,
        cache_latent,
        cache_rope,
        cache_lengths,
        expert_ids,
        route_weight,
        (attn_gain, q_gain, kv_gain, moe_gain),
        (w_qdown, w_kvdown, w_krope.T, w_qup, w_kup, w_vup, w_out),
        (expert_gate[0], expert_up[0], expert_down[0]),
        half_count,
    )
    block = send.shape[2]
    send = send.reshape(half_count, block, LANES)
    own = lax.all_to_all(send, "ep", split_axis=0, concat_axis=0, tiled=True)
    other = partner(own, "ep", 0)
    side = (lax.axis_index("ep") % 2).reshape(1).astype(jnp.int32)
    flat = (half_count * block, LANES)
    keep, give = run_expert(
        side, own.reshape(flat), other.reshape(flat), *experts
    )
    given = partner(give, "ep", 0)
    pair_sum = (keep.astype(F32) + given.astype(F32)).astype(BF16)
    returned = lax.all_to_all(
        pair_sum.reshape(half_count, block, LANES), "ep", split_axis=0, concat_axis=0, tiled=True
    )
    mixed = run_combine(mixed_attn, combine, returned.reshape(half_count // 2, 2, block, LANES))
    return (mixed, new_latent, new_rope_key)


def solution(mesh):
    placed = (
        P("ep", None),
        P("ep", None, None),
        P("ep", None, None),
        P("ep"),
        P("ep", None),
        P("ep", None),
        P(),
        P(),
        P(),
        P(),
        P(),
        P(),
        P(),
        P(),
        P(),
        P(),
        P(),
        P("ep", None, None),
        P("ep", None, None),
        P("ep", None, None),
    )
    return jax.shard_map(
        shards,
        mesh=mesh,
        in_specs=placed,
        out_specs=(P("ep", None), P("ep", None), P("ep", None)),
        check_vma=False,
    )
```

time: 108 us -> 55.8 us (0.52)
  matrix products: 35.1 us -> 0 us
  waiting for transfers between devices: 28.5 us -> 3.26 us
  Pallas kernels: 0 us -> 18.1 us
  blocking collectives: 21.2 us -> 33.3 us
  other arithmetic: 10.6 us -> 0.09 us
  local copies, waits for them, and re-layouts: 6.36 us -> 0.01 us
  starting transfers between devices: 3.18 us -> 0.2 us
    dot_general x19 -> x0, matrix products: 35.1 us -> none  [the longest x2 9.26 us: block_step(): jnp.einsum('thc,tpc->thp', q_latent, latent_block, preferred_element_type...]
    all_to_all x1 -> x0, waiting for transfers between devices: 24.8 us -> none  [mix_experts(): lax.all_to_all(pair_sum, 'ep', split_axis=0, concat_axis=0, tiled=True)]
    pallas_call x0 -> x3, Pallas kernels: none -> 18.1 us  [the longest x1 15.1 us: run_mixer(): pl.pallas_call(mixer(n_seq, n_pos, width, lat, expert_count, slot_count),...]
    all_to_all x1 -> x2, blocking collectives: 21.2 us -> 33.3 us  [the longest x1 19.2 us: shards(): own = lax.all_to_all(send, 'ep', split_axis=0, concat_axis=0, tiled=True)]
    reshape x5 -> x0, local copies, waits for them, and re-layouts: 4.32 us -> none  [the longest x1 1.4 us: mix_experts(): flat_rows = slot_rows.reshape(-1, model_width)]
    all_to_all x1 -> x0, starting transfers between devices: 2.97 us -> none  [mix_experts(): lax.all_to_all(pair_sum, 'ep', split_axis=0, concat_axis=0, tiled=True)]
    concatenate x4 -> x0, other arithmetic: 2.34 us -> none  [the longest x1 1.5 us: mix_experts(): slot_rows = jnp.concatenate([own_rows, sibling], axis=1)]
    add x8 -> x0, other arithmetic: 2.1 us -> none  [the longest x1 1.33 us: mix_experts(): outputs[:, :per_core].astype(jnp.float32) + from_sibling.astype(jnp.float32)]
  transfers between devices with their start and end apart: 3 -> 2, of which waited for: 3 -> 2; matrix products, arithmetic and copies ran while one was open for 1% -> 0% of each run, Pallas kernels for 0% -> 0%
where the time goes in v1:
time: 55.8 us; the launch traced here: 55.6 us
  blocking collectives  33.3 us (60%)
  Pallas kernels  18.1 us (32%)
  waiting for transfers between devices  3.26 us (6%)
  between operations  0.66 us (1%)
    all_to_all x1, blocking collectives, shards(): own = lax.all_to_all(send, 'ep', split_axis=0, concat_axis=0, tiled=True)  19.2 us
    pallas_call x1, Pallas kernels, run_mixer(): pl.pallas_call(mixer(n_seq, n_pos, width, lat, expert_count, slot_count),...  15.1 us
    all_to_all x1, blocking collectives, shards(): lax.all_to_all(pair_sum.reshape(half_count, block, LANES), 'ep', split_ax...  14.2 us
    ppermute x2, waiting for transfers between devices, partner(): return lax.ppermute(value, axis, pairs)  3.26 us
    pallas_call x1, Pallas kernels, run_expert(): pl.pallas_call(expert_kernel(count // chunks, chunks), out_shape=(jax.Sha...  2.03 us
  transfers between devices with their start and end apart: 2, of which 2 were waited for; matrix products, arithmetic and copies ran while one was open for 0% of the time, Pallas kernels for 0%

profile of v1, /device:TPU:0, one launch (start us, length us, event | category | flops | bytes accessed | tf_op | source)
XLA Modules:
  0.0 55.6 jit_solution(14740237161569170371)
XLA Ops:
  0.6 15.1 %mixer.1 = (f32[12,2048]{1,0:T(8,128)}, bf16[12,512]{1,0:T(8,128)(2,1)}, bf16[12,64]{1,0:T(8,128)(2,1)}, bf16[16,2,40,128]{3,2,1,0:T(8,128)(2,1)S(1)}, bf16[2,12...) custom-call(s32[12]{0:T(128)} %len_hbm.1, ...), custom_call_target="tpu_custom_call" | custom-call | tf_op jit(solution)/shard_map/mixer/pallas_call | solution.py:363
  15.7 19.2 %all_to_all.10 = bf16[32,40,128]{2,1,0:T(8,128)(2,1)S(1)} all-to-all(bf16[32,40,128]{2,1,0:T(8,128)(2,1)S(1)} %bitcast.19), channel_id=1, replica_groups=mesh['ep'=32] {'ep'}, dimensions={0} | all-to-all | bytes 655360 | tf_op jit(solution)/shard_map/all_to_all | solution.py:511
  34.9 0.0 collective-permute-start
  34.9 1.8 %collective-permute-done = bf16[32,40,128]{2,1,0:T(8,128)(2,1)} collective-permute-done((bf16[32,40,128]{2,1,0:T(8,128)(2,1)S(1)}, bf16[32,40,128]{2,1,0:T(8,128)(2,1)}, u32[]{:S(2)}, u32[]{:S(2)}) %collective-permute-start) | collective-permute-done | bytes 327712 | tf_op jit(solution)/shard_map/ppermute | solution.py:38
  36.6 0.0 copy-start
  36.7 0.0 copy-start.1
  36.7 2.0 %expert_half.1 = (bf16[1280,128]{1,0:T(8,128)(2,1)S(1)}, bf16[1280,128]{1,0:T(8,128)(2,1)S(1)}) custom-call(s32[1]{0:T(128)} %bitcast.11.side_ref, bf16[1280,128]{1,0:T(8,128)(2,1)S(1)} %bitcast.18, bf16[1280,128]{1,0:T(8,128)(2,1)} %bitcast.14.other_ref, bf16[2048,256]{1,0:T(8,128)(2,1)S(1)} %get-tuple-element.16.gate_ref, ...), custom_call_target="tpu_custom_call" | custom-call | tf_op jit(solution)/shard_map/expert_half/pallas_call | solution.py:435
  38.7 0.2 collective-permute-start.1
  38.9 1.5 %collective-permute-done.1 = bf16[1280,128]{1,0:T(8,128)(2,1)S(1)} collective-permute-done((bf16[1280,128]{1,0:T(8,128)(2,1)S(1)}, bf16[1280,128]{1,0:T(8,128)(2,1)S(1)}, u32[]{:S(2)}, u32[]{:S(2)}) %collective-permute-start.1) | collective-permute-done | bytes 327712 | tf_op jit(solution)/shard_map/ppermute | solution.py:38
  40.4 0.1 add_convert_fusion
  40.5 14.2 %all_to_all.11 = bf16[32,40,128]{2,1,0:T(8,128)(2,1)S(1)} all-to-all(bf16[32,40,128]{2,1,0:T(8,128)(2,1)S(1)} %bitcast.21), channel_id=1, replica_groups=mesh['ep'=32] {'ep'}, dimensions={0} | all-to-all | bytes 655360 | tf_op jit(solution)/shard_map/all_to_all | solution.py:520
  54.6 0.0 copy-done
  54.6 0.0 copy-done.1
  54.7 1.0 %combine.1 = f32[12,2048]{1,0:T(8,128)} custom-call(f32[12,2048]{1,0:T(8,128)S(1)} %copy-done.1, bf16[2,128,640]{2,1,0:T(8,128)(2,1)S(1)} %copy-done, bf16[16,2,40,128]{3,2,1,0:T(8,128)(2,1)S(1)} %bitcast.17), custom_call_target="tpu_custom_call" | custom-call | tf_op jit(solution)/shard_map/combine/pallas_call | solution.py:464
Async XLA Ops:
  34.9 1.8 %collective-permute-start = (bf16[32,40,128]{2,1,0:T(8,128)(2,1)S(1)}, bf16[32,40,128]{2,1,0:T(8,128)(2,1)}, u32[]{:S(2)}, u32[]{:S(2)}) collective-permute-start(bf16[32,40,128]{2,1,0:T(8,128)(2,1)S(1)} %all_to_all.10), channel_id=1, source_target_pairs={{0,1},{1,0},{2,3},{3,2},{4,5},{5,4},{6,7},{7,6},{8,9},{9,8},{10,11... | collective-permute-start | bytes 983048 | tf_op jit(solution)/shard_map/ppermute | solution.py:38
  36.6 18.0 %copy-start = (bf16[2,128,640]{2,1,0:T(8,128)(2,1)S(1)}, bf16[2,128,640]{2,1,0:T(8,128)(2,1)}, u32[]{:S(2)}) copy-start(bf16[2,128,640]{2,1,0:T(8,128)(2,1)} %get-tuple-element.14.combine_ref) | copy-start | bytes 983044
  36.7 18.0 %copy-start.1 = (f32[12,2048]{1,0:T(8,128)S(1)}, f32[12,2048]{1,0:T(8,128)}, u32[]{:S(2)}) copy-start(f32[12,2048]{1,0:T(8,128)} %get-tuple-element.13.mixed_ref) | copy-start | bytes 294916
  38.7 1.7 %collective-permute-start.1 = (bf16[1280,128]{1,0:T(8,128)(2,1)S(1)}, bf16[1280,128]{1,0:T(8,128)(2,1)S(1)}, u32[]{:S(2)}, u32[]{:S(2)}) collective-permute-start(bf16[1280,128]{1,0:T(8,128)(2,1)S(1)} %get-tuple-element.20), channel_id=1, source_target_pairs={{0,1},{1,0},{2,3},{3,2},{4,5},{5,4},{6,7},{7,6},{8,9},{9,8},{10,11... | collective-permute-start | bytes 983048 | tf_op jit(solution)/shard_map/ppermute | solution.py:38

commit v2 on v1

--- a/solution.py
+++ b/solution.py
@@ -16,7 +16,8 @@
 LANES = 128
 ROWS = 16
 SEQ_STEP = 4
-SEQ_AHEAD = 8
+GROUPS_AHEAD = 3
+BLOCK_POS = 256
 
 EPS = 1e-06
 THETA = 10000.0
@@ -109,6 +110,11 @@
         w_out,
         latent,
         rope,
+        order_s,
+        blocks_s,
+        score_s,
+        prob_s,
+        sum_s,
         q_lat_s,
         q_rope_s,
         o_lat_s,
@@ -155,22 +161,57 @@
             ]
             return pltpu.make_async_copy(pairs[i][0], pairs[i][1], w_sem.at[i])
 
-        def latent_copy(t):
-            return pltpu.make_async_copy(latent_hbm.at[t], latent.at[t], c_sem.at[t])
-
-        def rope_copy(t):
-            return pltpu.make_async_copy(rope_hbm.at[t], rope.at[t], r_sem.at[t])
-
-        def cache_start(t):
-            latent_copy(t).start()
-            rope_copy(t).start()
+        group_count = n_seq // SEQ_STEP
+        most_blocks = pl.cdiv(n_pos, BLOCK_POS)
+
+        def latent_copy(group, j, block):
+            slot = group * SEQ_STEP + j
+            rows = pl.ds(block * BLOCK_POS, min(BLOCK_POS, n_pos - block * BLOCK_POS))
+            return pltpu.make_async_copy(
+                latent_hbm.at[order_s[slot], rows, :],
+                latent.at[slot, rows, :],
+                c_sem.at[slot, block],
+            )
+
+        def rope_copy(group, j):
+            slot = group * SEQ_STEP + j
+            return pltpu.make_async_copy(rope_hbm.at[order_s[slot]], rope.at[slot], r_sem.at[slot])
+
+        def each_copy(group, act):
+            for block in range(most_blocks):
+
+                @pl.when(blocks_s[group] > block)
+                def _(block=block):
+                    for j in range(SEQ_STEP):
+                        act(latent_copy(group, j, block))
+
+            for j in range(SEQ_STEP):
+                act(rope_copy(group, j))
+
+        def cache_start(group):
+            each_copy(group, lambda copy: copy.start())
 
         weight_copy(0).start()
         weight_copy(1).start()
 
+        small[2].wait()
+        lengths = [len_ref[t] for t in range(n_seq)]
+        places = [jnp.int32(0)] * n_seq
+        for i in range(n_seq):
+            for j in range(i):
+                later = (lengths[i] > lengths[j]).astype(jnp.int32)
+                places[j] = places[j] + later
+                places[i] = places[i] + (1 - later)
+        for t in range(n_seq):
+            order_s[places[t]] = jnp.int32(t)
+        for group in range(group_count):
+            longest = len_ref[order_s[group * SEQ_STEP]]
+            blocks_s[group] = (longest + (BLOCK_POS - 1)) // BLOCK_POS
+
         expert_row = lax.broadcasted_iota(jnp.int32, (expert_count, LANES), 0)
-        for copy in small:
-            copy.wait()
+        for i, copy in enumerate(small):
+            if i != 2:
+                copy.wait()
         token_lane = lax.broadcasted_iota(jnp.int32, (n_seq, LANES), 1)
         token_row = lax.broadcasted_iota(jnp.int32, (n_seq, LANES), 0)
         spread = (token_lane % ROWS == token_row).astype(BF16)
@@ -214,11 +255,9 @@
         normed = norm_gain(tokens, attn_gain_ref[...]).astype(BF16)
         weight_copy(0).wait()
         cache_start(0)
-        cache_start(1)
         q_low = norm_gain(mm(normed, qdown[...]), q_gain_ref[...]).astype(BF16)
         weight_copy(1).wait()
-        cache_start(2)
-        cache_start(3)
+        cache_start(1)
         new_latent = norm_gain(mm(normed, kvdown[...]), kv_gain_ref[...]).astype(BF16)
         new_latent_ref[...] = new_latent
         latent_row_s[...] = new_latent.astype(F32)
@@ -250,8 +289,8 @@
         key_row_s[...] = jnp.where(low_half, new_key.astype(F32), 0.0)
 
         weight_copy(3).wait()
-        for t in range(4, SEQ_AHEAD):
-            cache_start(t)
+        for group in range(2, GROUPS_AHEAD):
+            cache_start(group)
         query = mm(q_low, qup[...])
         weight_copy(4).wait()
         for pair in range(HEADS // 2):
@@ -271,47 +310,78 @@
                 turned = both if side == 0 else pltpu.roll(both, ROPE_DIM, 1)
                 q_rope_s[:, head, :] = turned
 
-        position = lax.broadcasted_iota(jnp.int32, (HEADS, n_pos), 1)
-
-        def step(group, carry):
-            start = group * SEQ_STEP
+        def for_blocks(group, act):
+            for block in range(most_blocks):
+
+                @pl.when(blocks_s[group] == block + 1)
+                def _(count=min(n_pos, (block + 1) * BLOCK_POS)):
+                    act(group, count)
+
+        def score(group, count):
             for j in range(SEQ_STEP):
-
-                @pl.when(start + j + SEQ_AHEAD < n_seq)
-                def _(ahead=start + j + SEQ_AHEAD):
-                    cache_start(ahead)
-
-            @pl.when((start + SEQ_AHEAD >= n_seq) & (start + SEQ_AHEAD < n_seq + SEQ_STEP))
-            def _():
-                for i in range(5, 10):
-                    weight_copy(i).start()
-
-            for j in range(SEQ_STEP):
-                latent_copy(start + j).wait()
-                rope_copy(start + j).wait()
-            for j in range(SEQ_STEP):
-                t = start + j
+                slot = group * SEQ_STEP + j
+                t = order_s[slot]
                 q_lat = q_lat_s[t].astype(BF16)
                 q_rope = q_rope_s[t].astype(BF16)
-                own_row = latent_row_s[pl.ds(t, 1), :]
-                own_key = key_row_s[pl.ds(t, 1), :]
-                own = (
-                    jnp.sum(q_lat.astype(F32) * own_row, axis=1, keepdims=True)
-                    + jnp.sum(q_rope.astype(F32) * own_key, axis=1, keepdims=True)
-                ) * scale
-                scores = (
-                    mm_t(q_lat, latent[t]) + mm(q_rope[:, :ROPE_DIM], rope[t])
-                ) * scale
-                scores = jnp.where(position < len_ref[t], scores, -jnp.inf)
-                peak = jnp.maximum(jnp.max(scores, axis=1, keepdims=True), own)
-                probs = jnp.exp(scores - peak)
-                own_prob = jnp.exp(own - peak)
-                total = jnp.sum(probs, axis=1, keepdims=True) + own_prob
-                summed = mm(probs.astype(BF16), latent[t]) + own_prob.astype(BF16).astype(F32) * own_row
-                o_lat_s[:, pl.ds(t, 1), :] = (summed / total)[:, None, :]
+                score_s[slot, :, :count] = mm_t(q_lat, latent[slot, :count, :]) + mm(
+                    q_rope[:, :ROPE_DIM], rope[slot, :, :count]
+                )
+
+        def weigh(group, count):
+            for j in range(SEQ_STEP):
+                slot = group * SEQ_STEP + j
+                sum_s[slot] = mm(prob_s[slot, :, :count].astype(BF16), latent[slot, :count, :])
+
+        def score_step(group, carry):
+            @pl.when(group + GROUPS_AHEAD < group_count)
+            def _():
+                cache_start(group + GROUPS_AHEAD)
+
+            each_copy(group, lambda copy: copy.wait())
+
+            @pl.when(group == 0)
+            def _():
+                weight_copy(5).start()
+                weight_copy(6).start()
+
+            @pl.when(group == group_count - 1)
+            def _():
+                for i in range(7, 10):
+                    weight_copy(i).start()
+
+            for_blocks(group, score)
             return carry
 
-        lax.fori_loop(0, n_seq // SEQ_STEP, step, 0)
+        def weigh_step(group, carry):
+            for_blocks(group, weigh)
+            return carry
+
+        lax.fori_loop(0, group_count, score_step, 0)
+
+        position = lax.broadcasted_iota(jnp.int32, (HEADS, n_pos), 1)
+        ends = []
+        for slot in range(n_seq):
+            t = order_s[slot]
+            own_row = latent_row_s[pl.ds(t, 1), :]
+            own_key = key_row_s[pl.ds(t, 1), :]
+            own = (
+                jnp.sum(q_lat_s[t].astype(BF16).astype(F32) * own_row, axis=1, keepdims=True)
+                + jnp.sum(q_rope_s[t].astype(BF16).astype(F32) * own_key, axis=1, keepdims=True)
+            ) * scale
+            scores = jnp.where(position < len_ref[t], score_s[slot] * scale, -jnp.inf)
+            peak = jnp.maximum(jnp.max(scores, axis=1, keepdims=True), own)
+            probs = jnp.exp(scores - peak)
+            own_prob = jnp.exp(own - peak)
+            ends.append((own_prob, jnp.sum(probs, axis=1, keepdims=True) + own_prob))
+            prob_s[slot] = probs
+
+        lax.fori_loop(0, group_count, weigh_step, 0)
+
+        for slot, (own_prob, total) in enumerate(ends):
+            t = order_s[slot]
+            own_row = latent_row_s[pl.ds(t, 1), :]
+            summed = sum_s[slot] + own_prob.astype(BF16).astype(F32) * own_row
+            o_lat_s[:, pl.ds(t, 1), :] = (summed / total)[:, None, :]
 
         weight_copy(5).wait()
         parts = []
@@ -382,6 +452,11 @@
         + [
             pltpu.VMEM((n_seq, n_pos, lat), BF16),
             pltpu.VMEM((n_seq, ROPE_DIM, n_pos), BF16),
+            pltpu.SMEM((n_seq,), jnp.int32),
+            pltpu.SMEM((n_seq,), jnp.int32),
+            pltpu.VMEM((n_seq, HEADS, n_pos), F32),
+            pltpu.VMEM((n_seq, HEADS, n_pos), F32),
+            pltpu.VMEM((n_seq, HEADS, lat), F32),
             pltpu.VMEM((n_seq, HEADS, lat), F32),
             pltpu.VMEM((n_seq, HEADS, LANES), F32),
             pltpu.VMEM((HEADS, n_seq, lat), F32),
@@ -389,7 +464,7 @@
             pltpu.VMEM((n_seq, lat), F32),
             pltpu.VMEM((n_seq, LANES), F32),
             pltpu.SemaphoreType.DMA((len(mats) + len(experts),)),
-            pltpu.SemaphoreType.DMA((n_seq,)),
+            pltpu.SemaphoreType.DMA((n_seq, pl.cdiv(n_pos, BLOCK_POS))),
             pltpu.SemaphoreType.DMA((n_seq,)),
             pltpu.SemaphoreType.DMA((len(small),)),
             pltpu.SemaphoreType.DMA((2,)),
@@ -438,9 +513,9 @@
         in_specs=[pl.BlockSpec(memory_space=pltpu.SMEM)] + [vmem] * 5,
         out_specs=(vmem, vmem),
         scratch_shapes=[pltpu.VMEM((2, count, LANES), F32)],
-        compiler_params=pltpu.CompilerParams(vmem_limit_bytes=40 * 1024 * 1024),
+        compiler_params=pltpu.CompilerParams(vmem_limit_bytes=12 * 1024 * 1024),
         name="expert_half",
-    )(side, own, other, gate, up, down)
+    )(side, own, pltpu.with_memory_space_constraint(other, pltpu.VMEM), gate, up, down)
 
 
 def combine_kernel(n_seq, chunks):
@@ -466,7 +541,7 @@
         out_shape=jax.ShapeDtypeStruct(mixed.shape, F32),
         in_specs=[vmem] * 3,
         out_specs=vmem,
-        compiler_params=pltpu.CompilerParams(vmem_limit_bytes=40 * 1024 * 1024),
+        compiler_params=pltpu.CompilerParams(vmem_limit_bytes=12 * 1024 * 1024),
         name="combine",
     )(mixed, combine, rows)
 
@@ -509,12 +584,10 @@
     block = send.shape[2]
     send = send.reshape(half_count, block, LANES)
     own = lax.all_to_all(send, "ep", split_axis=0, concat_axis=0, tiled=True)
+    own = own.reshape(half_count * block, LANES)
     other = partner(own, "ep", 0)
     side = (lax.axis_index("ep") % 2).reshape(1).astype(jnp.int32)
-    flat = (half_count * block, LANES)
-    keep, give = run_expert(
-        side, own.reshape(flat), other.reshape(flat), *experts
-    )
+    keep, give = run_expert(side, own, other, *experts)
     given = partner(give, "ep", 0)
     pair_sum = (keep.astype(F32) + given.astype(F32)).astype(BF16)
     returned = lax.all_to_all(

time: 55.8 us -> 52.7 us (0.944)
  Pallas kernels: 18.1 us -> 14.8 us
    pallas_call x1, Pallas kernels: 15.1 us -> 11.8 us  [run_mixer(): pl.pallas_call(mixer(n_seq, n_pos, width, lat, expert_count, slot_count),...]
where the time goes in v2:
time: 52.7 us; the launch traced here: 52.6 us
  blocking collectives  33.5 us (64%)
  Pallas kernels  14.8 us (28%)
  waiting for transfers between devices  3.26 us (6%)
  between operations  0.66 us (1%)
    all_to_all x1, blocking collectives, shards(): own = lax.all_to_all(send, 'ep', split_axis=0, concat_axis=0, tiled=True)  19.3 us
    all_to_all x1, blocking collectives, shards(): lax.all_to_all(pair_sum.reshape(half_count, block, LANES), 'ep', split_ax...  14.2 us
    pallas_call x1, Pallas kernels, run_mixer(): pl.pallas_call(mixer(n_seq, n_pos, width, lat, expert_count, slot_count),...  11.8 us
    ppermute x2, waiting for transfers between devices, partner(): return lax.ppermute(value, axis, pairs)  3.26 us
    pallas_call x1, Pallas kernels, run_expert(): pl.pallas_call(expert_kernel(count // chunks, chunks), out_shape=(jax.Sha...  2.03 us
  transfers between devices with their start and end apart: 2, of which 2 were waited for; matrix products, arithmetic and copies ran while one was open for 0% of the time, Pallas kernels for 0%

profile of v2, /device:TPU:0, one launch (start us, length us, event | category | flops | bytes accessed | tf_op | source)
XLA Modules:
  0.0 52.6 jit_solution(2312384563804521298)
XLA Ops:
  0.6 11.8 %mixer.1 = (f32[12,2048]{1,0:T(8,128)}, bf16[12,512]{1,0:T(8,128)(2,1)}, bf16[12,64]{1,0:T(8,128)(2,1)}, bf16[16,2,40,128]{3,2,1,0:T(8,128)(2,1)S(1)}, bf16[2,12...) custom-call(s32[12]{0:T(128)} %len_hbm.1, ...), custom_call_target="tpu_custom_call" | custom-call | tf_op jit(solution)/shard_map/mixer/pallas_call | solution.py:433
  12.5 19.3 %all_to_all.10 = bf16[32,40,128]{2,1,0:T(8,128)(2,1)S(1)} all-to-all(bf16[32,40,128]{2,1,0:T(8,128)(2,1)S(1)} %bitcast.19), channel_id=1, replica_groups=mesh['ep'=32] {'ep'}, dimensions={0} | all-to-all | bytes 655360 | tf_op jit(solution)/shard_map/all_to_all | solution.py:586
  31.8 0.0 collective-permute-start
  31.8 1.8 %collective-permute-done.other_ref = bf16[1280,128]{1,0:T(8,128)(2,1)} collective-permute-done((bf16[1280,128]{1,0:T(8,128)(2,1)S(1)}, bf16[1280,128]{1,0:T(8,128)(2,1)}, u32[]{:S(2)}, u32[]{:S(2)}) %collective-permute-start) | collective-permute-done | bytes 327712 | tf_op jit(solution)/shard_map/ppermute | solution.py:39
  33.6 0.0 copy-start
  33.6 0.0 copy-start.1
  33.6 2.0 %expert_half.1 = (bf16[1280,128]{1,0:T(8,128)(2,1)S(1)}, bf16[1280,128]{1,0:T(8,128)(2,1)S(1)}) custom-call(s32[1]{0:T(128)} %bitcast.11.side_ref, bf16[1280,128]{1,0:T(8,128)(2,1)S(1)} %bitcast.18, bf16[1280,128]{1,0:T(8,128)(2,1)} %collective-permute-done.other_ref, bf16[2048,256]{1,0:T(8,128)(2,1)S(1)} %get-tuple-element.16.gate_ref, ...), custom_call_target="tpu_custom_call" | custom-call | tf_op jit(solution)/shard_map/expert_half/pallas_call | solution.py:510
  35.6 0.2 collective-permute-start.1
  35.8 1.5 %collective-permute-done.1 = bf16[1280,128]{1,0:T(8,128)(2,1)S(1)} collective-permute-done((bf16[1280,128]{1,0:T(8,128)(2,1)S(1)}, bf16[1280,128]{1,0:T(8,128)(2,1)S(1)}, u32[]{:S(2)}, u32[]{:S(2)}) %collective-permute-start.1) | collective-permute-done | bytes 327712 | tf_op jit(solution)/shard_map/ppermute | solution.py:39
  37.3 0.1 add_convert_fusion
  37.4 14.2 %all_to_all.11 = bf16[32,40,128]{2,1,0:T(8,128)(2,1)S(1)} all-to-all(bf16[32,40,128]{2,1,0:T(8,128)(2,1)S(1)} %bitcast.21), channel_id=1, replica_groups=mesh['ep'=32] {'ep'}, dimensions={0} | all-to-all | bytes 655360 | tf_op jit(solution)/shard_map/all_to_all | solution.py:593
  51.6 0.0 copy-done
  51.6 0.0 copy-done.1
  51.6 1.0 %combine.1 = f32[12,2048]{1,0:T(8,128)} custom-call(f32[12,2048]{1,0:T(8,128)S(1)} %copy-done.1, bf16[2,128,640]{2,1,0:T(8,128)(2,1)S(1)} %copy-done, bf16[16,2,40,128]{3,2,1,0:T(8,128)(2,1)S(1)} %bitcast.16), custom_call_target="tpu_custom_call" | custom-call | tf_op jit(solution)/shard_map/combine/pallas_call | solution.py:539
Async XLA Ops:
  31.8 1.8 %collective-permute-start = (bf16[1280,128]{1,0:T(8,128)(2,1)S(1)}, bf16[1280,128]{1,0:T(8,128)(2,1)}, u32[]{:S(2)}, u32[]{:S(2)}) collective-permute-start(bf16[1280,128]{1,0:T(8,128)(2,1)S(1)} %bitcast.17), channel_id=1, source_target_pairs={{0,1},{1,0},{2,3},{3,2},{4,5},{5,4},{6,7},{7,6},{8,9},{9,8},{10,11... | collective-permute-start | bytes 983048 | tf_op jit(solution)/shard_map/ppermute | solution.py:39
  33.6 18.0 %copy-start = (bf16[2,128,640]{2,1,0:T(8,128)(2,1)S(1)}, bf16[2,128,640]{2,1,0:T(8,128)(2,1)}, u32[]{:S(2)}) copy-start(bf16[2,128,640]{2,1,0:T(8,128)(2,1)} %get-tuple-element.14.combine_ref) | copy-start | bytes 983044
  33.6 18.0 %copy-start.1 = (f32[12,2048]{1,0:T(8,128)S(1)}, f32[12,2048]{1,0:T(8,128)}, u32[]{:S(2)}) copy-start(f32[12,2048]{1,0:T(8,128)} %get-tuple-element.13.mixed_ref) | copy-start | bytes 294916
  35.6 1.7 %collective-permute-start.1 = (bf16[1280,128]{1,0:T(8,128)(2,1)S(1)}, bf16[1280,128]{1,0:T(8,128)(2,1)S(1)}, u32[]{:S(2)}, u32[]{:S(2)}) collective-permute-start(bf16[1280,128]{1,0:T(8,128)(2,1)S(1)} %get-tuple-element.20), channel_id=1, source_target_pairs={{0,1},{1,0},{2,3},{3,2},{4,5},{5,4},{6,7},{7,6},{8,9},{9,8},{10,11... | collective-permute-start | bytes 983048 | tf_op jit(solution)/shard_map/ppermute | solution.py:39

commit v3 on v2

--- a/solution.py
+++ b/solution.py
@@ -61,6 +61,7 @@
     chunks = half // LANES
 
     def body(
+        side_ref,
         len_hbm,
         tokens_hbm,
         inverse_hbm,
@@ -90,6 +91,7 @@
         gate_ref,
         up_ref,
         down_ref,
+        give_ref,
         len_ref,
         tokens_ref,
         inverse_ref,
@@ -127,6 +129,11 @@
         s_sem,
         o_sem,
     ):
+        side = side_ref[0]
+        hidden = gate_hbm.shape[1]
+        here = pl.ds(pl.multiple_of(side * half, half), half)
+        there = pl.ds(pl.multiple_of((1 - side) * half, half), half)
+        weight_count = 12 + half // hidden
         small = [
             pltpu.make_async_copy(source, target, s_sem.at[i])
             for i, (source, target) in enumerate(
@@ -155,10 +162,16 @@
                 (kup_hbm, kup),
                 (vup_hbm, vup),
                 (out_hbm, w_out),
-                (gate_hbm, gate_ref),
-                (up_hbm, up_ref),
-                (down_hbm, down_ref),
+                (gate_hbm.at[here, :], gate_ref),
+                (up_hbm.at[here, :], up_ref),
+                (down_hbm.at[:, here], down_ref),
+                (gate_hbm.at[there, :], give_ref.at[:half, :]),
+                (up_hbm.at[there, :], give_ref.at[half : 2 * half, :]),
             ]
+            for b in range(half // hidden):
+                cols = slice(b * hidden, (b + 1) * hidden)
+                rows = slice(2 * half + b * hidden, 2 * half + (b + 1) * hidden)
+                pairs.append((down_hbm.at[:, there].at[:, cols], give_ref.at[rows, :]))
             return pltpu.make_async_copy(pairs[i][0], pairs[i][1], w_sem.at[i])
 
         group_count = n_seq // SEQ_STEP
@@ -346,7 +359,7 @@
 
             @pl.when(group == group_count - 1)
             def _():
-                for i in range(7, 10):
+                for i in range(7, weight_count):
                     weight_copy(i).start()
 
             for_blocks(group, score)
@@ -394,7 +407,7 @@
             )
         heads_out = jnp.concatenate(parts, axis=1)
         weight_copy(6).wait()
-        for i in range(7, 10):
+        for i in range(7, weight_count):
             weight_copy(i).wait()
         mixed = (tokens + mm(heads_out, w_out[...])).astype(BF16).astype(F32)
         mixed_ref[...] = mixed
@@ -413,12 +426,14 @@
     return body
 
 
-def run_mixer(tokens, cache_latent, cache_rope, cache_lengths, ids, weights, gains, mats, experts, half_count):
+def run_mixer(side, tokens, cache_latent, cache_rope, cache_lengths, ids, weights, gains, mats, experts, half_count):
     n_seq, width = tokens.shape
     _, n_pos, lat = cache_latent.shape
     expert_count = half_count // 2
     slot_count = capacity_of(half_count)
-    chunks = width // 2 // LANES
+    half = width // 2
+    hidden = experts[0].shape[1]
+    chunks = half // LANES
     rows_per = slot_count * chunks
     vmem = pl.BlockSpec(memory_space=pltpu.VMEM)
     hbm = pl.BlockSpec(memory_space=pltpu.HBM)
@@ -438,10 +453,13 @@
             jax.ShapeDtypeStruct((n_seq, ROPE_DIM), BF16),
             jax.ShapeDtypeStruct((expert_count, 2, rows_per, LANES), BF16),
             pltpu.HBM((2, LANES, expert_count * rows_per), BF16),
-            *[jax.ShapeDtypeStruct(m.shape, BF16) for m in experts],
+            jax.ShapeDtypeStruct((half, hidden), BF16),
+            jax.ShapeDtypeStruct((half, hidden), BF16),
+            jax.ShapeDtypeStruct((hidden, half), BF16),
+            jax.ShapeDtypeStruct((3 * half, hidden), BF16),
         ),
-        in_specs=[hbm] * (len(small) + len(mats) + 2 + len(experts)),
-        out_specs=(hbm, vmem, vmem, vmem, hbm) + (vmem,) * len(experts),
+        in_specs=[pl.BlockSpec(memory_space=pltpu.SMEM)] + [hbm] * (len(small) + len(mats) + 2 + len(experts)),
+        out_specs=(hbm, vmem, vmem, vmem, hbm) + (vmem,) * 4,
         scratch_shapes=[pltpu.SMEM((n_seq,), jnp.int32)]
         + [pltpu.VMEM(m.shape, m.dtype) for m in small[1:]]
         + [
@@ -463,7 +481,7 @@
             pltpu.VMEM((2, chunks * ROWS, LANES), F32),
             pltpu.VMEM((n_seq, lat), F32),
             pltpu.VMEM((n_seq, LANES), F32),
-            pltpu.SemaphoreType.DMA((len(mats) + len(experts),)),
+            pltpu.SemaphoreType.DMA((12 + half // hidden,)),
             pltpu.SemaphoreType.DMA((n_seq, pl.cdiv(n_pos, BLOCK_POS))),
             pltpu.SemaphoreType.DMA((n_seq,)),
             pltpu.SemaphoreType.DMA((len(small),)),
@@ -472,6 +490,7 @@
         compiler_params=pltpu.CompilerParams(vmem_limit_bytes=44 * 1024 * 1024),
         name="mixer",
     )(
+        side,
         *[
             pltpu.with_memory_space_constraint(m, pltpu.HBM)
             for m in (*small, *mats, cache_latent, jnp.swapaxes(cache_rope, 1, 2), *experts)
@@ -479,43 +498,79 @@
     )
 
 
-def expert_kernel(rows, chunks):
+def inner_kernel(rows, chunks, hidden):
     half = chunks * LANES
 
-    def body(side_ref, own_ref, other_ref, gate_ref, up_ref, down_ref, keep_ref, pass_ref, wide):
-        side = side_ref[0]
-        halves = []
-        for slot, ref in ((0, own_ref), (1, other_ref)):
-            wide[slot] = ref[...].astype(F32)
-            cols = [wide[slot, pl.ds(r, rows, stride=chunks), :].astype(BF16) for r in range(chunks)]
-            halves.append(jnp.concatenate(cols, axis=1))
-        here = pl.ds(pl.multiple_of(side * half, half), half)
-        there = pl.ds(pl.multiple_of((1 - side) * half, half), half)
-        gate = mm(halves[0], gate_ref[here, :]) + mm(halves[1], gate_ref[there, :])
-        up = mm(halves[0], up_ref[here, :]) + mm(halves[1], up_ref[there, :])
-        hidden = (gate * jax.nn.sigmoid(gate) * up).astype(BF16)
-        for slot, cols, ref in ((0, there, pass_ref), (1, here, keep_ref)):
-            out = mm(hidden, down_ref[:, cols])
-            for r in range(chunks):
-                wide[slot, pl.ds(r, rows, stride=chunks), :] = out[:, r * LANES : (r + 1) * LANES]
-            ref[...] = wide[slot].astype(BF16)
+    def body(own_ref, gate_ref, up_ref, other_ref, keep_ref, give_ref, wide):
+        wide[...] = own_ref[...].astype(F32)
+        cols = [wide[pl.ds(r, rows, stride=chunks), :].astype(BF16) for r in range(chunks)]
+        own = jnp.concatenate(cols, axis=1)
+        mats = (gate_ref[...], up_ref[...], other_ref[:half, :], other_ref[half : 2 * half, :])
+        for i, mat in enumerate(mats):
+            part = mm(own, mat)
+            keep_ref[:, i * hidden : (i + 1) * hidden] = part
+            place = (i + 2) % 4
+            give_ref[:, place * hidden : (place + 1) * hidden] = part.astype(BF16)
 
     return body
 
 
-def run_expert(side, own, other, gate, up, down):
+def run_inner(own, gate, up, other):
     count, _ = own.shape
-    chunks = gate.shape[0] // 2 // LANES
+    half, hidden = gate.shape
+    chunks = half // LANES
+    rows = count // chunks
     vmem = pl.BlockSpec(memory_space=pltpu.VMEM)
     return pl.pallas_call(
-        expert_kernel(count // chunks, chunks),
-        out_shape=(jax.ShapeDtypeStruct(own.shape, BF16),) * 2,
-        in_specs=[pl.BlockSpec(memory_space=pltpu.SMEM)] + [vmem] * 5,
+        inner_kernel(rows, chunks, hidden),
+        out_shape=(
+            jax.ShapeDtypeStruct((rows, 4 * hidden), F32),
+            jax.ShapeDtypeStruct((rows, 4 * hidden), BF16),
+        ),
+        in_specs=[vmem] * 4,
         out_specs=(vmem, vmem),
-        scratch_shapes=[pltpu.VMEM((2, count, LANES), F32)],
+        scratch_shapes=[pltpu.VMEM((count, LANES), F32)],
         compiler_params=pltpu.CompilerParams(vmem_limit_bytes=12 * 1024 * 1024),
-        name="expert_half",
-    )(side, own, pltpu.with_memory_space_constraint(other, pltpu.VMEM), gate, up, down)
+        name="expert_inner",
+    )(own, gate, up, other)
+
+
+def outer_kernel(rows, chunks, hidden):
+    half = chunks * LANES
+
+    def body(keep_ref, given_ref, down_ref, other_ref, out_ref, wide):
+        total = keep_ref[...] + given_ref[...].astype(F32)
+        acts = []
+        for start in (0, 2 * hidden):
+            gate = total[:, start : start + hidden]
+            up = total[:, start + hidden : start + 2 * hidden]
+            acts.append((gate * jax.nn.sigmoid(gate) * up).astype(BF16))
+        for b in range(half // hidden):
+            cols = slice(b * hidden, (b + 1) * hidden)
+            base = 2 * half + b * hidden
+            out = mm(acts[0], down_ref[:, cols]) + mm(acts[1], other_ref[base : base + hidden, :])
+            for r in range(hidden // LANES):
+                row = b * (hidden // LANES) + r
+                wide[pl.ds(row, rows, stride=chunks), :] = out[:, r * LANES : (r + 1) * LANES]
+        out_ref[...] = wide[...].astype(BF16)
+
+    return body
+
+
+def run_outer(keep, given, down, other):
+    rows, _ = keep.shape
+    hidden, half = down.shape
+    chunks = half // LANES
+    vmem = pl.BlockSpec(memory_space=pltpu.VMEM)
+    return pl.pallas_call(
+        outer_kernel(rows, chunks, hidden),
+        out_shape=jax.ShapeDtypeStruct((rows * chunks, LANES), BF16),
+        in_specs=[vmem] * 4,
+        out_specs=vmem,
+        scratch_shapes=[pltpu.VMEM((rows * chunks, LANES), F32)],
+        compiler_params=pltpu.CompilerParams(vmem_limit_bytes=12 * 1024 * 1024),
+        name="expert_outer",
+    )(keep, given, down, other)
 
 
 def combine_kernel(n_seq, chunks):
@@ -569,7 +624,9 @@
     expert_down,
 ):
     half_count = lax.axis_size("ep")
-    mixed_attn, new_latent, new_rope_key, send, combine, *experts = run_mixer(
+    side = jnp.bitwise_and(lax.axis_index("ep"), 1).reshape(1)
+    mixed_attn, new_latent, new_rope_key, send, combine, gate, up, down, give = run_mixer(
+        side,
         tokens,
         cache_latent,
         cache_rope,
@@ -582,16 +639,14 @@
         half_count,
     )
     block = send.shape[2]
-    send = send.reshape(half_count, block, LANES)
-    own = lax.all_to_all(send, "ep", split_axis=0, concat_axis=0, tiled=True)
-    own = own.reshape(half_count * block, LANES)
-    other = partner(own, "ep", 0)
-    side = (lax.axis_index("ep") % 2).reshape(1).astype(jnp.int32)
-    keep, give = run_expert(side, own, other, *experts)
-    given = partner(give, "ep", 0)
-    pair_sum = (keep.astype(F32) + given.astype(F32)).astype(BF16)
+    other = partner(give, "ep", 0)
+    own = lax.all_to_all(
+        send.reshape(half_count, block, LANES), "ep", split_axis=0, concat_axis=0, tiled=True
+    )
+    keep, inner = run_inner(own.reshape(half_count * block, LANES), gate, up, other)
+    outputs = run_outer(keep, partner(inner, "ep", 0), down, other)
     returned = lax.all_to_all(
-        pair_sum.reshape(half_count, block, LANES), "ep", split_axis=0, concat_axis=0, tiled=True
+        outputs.reshape(half_count, block, LANES), "ep", split_axis=0, concat_axis=0, tiled=True
     )
     mixed = run_combine(mixed_attn, combine, returned.reshape(half_count // 2, 2, block, LANES))
     return (mixed, new_latent, new_rope_key)

time: 52.7 us -> 51.2 us (0.972)
  blocking collectives: 33.5 us -> 35.7 us
  waiting for transfers between devices: 3.26 us -> 1.62 us
  Pallas kernels: 14.8 us -> 13.4 us
    all_to_all x2, blocking collectives: 33.5 us -> 35.7 us  [the longest x1 21.5 us: shards(): lax.all_to_all(send.reshape(half_count, block, LANES), 'ep', split_axis=0...]
    ppermute x2, waiting for transfers between devices: 3.26 us -> 1.62 us  [partner(): return lax.ppermute(value, axis, pairs)]
    pallas_call x1 -> x2, Pallas kernels: 2.03 us -> 0.95 us  [the longest x1 0.54 us: run_inner(): pl.pallas_call(inner_kernel(rows, chunks, hidden), out_shape=(jax.ShapeDt...]
  transfers between devices with their start and end apart: 2 -> 2, of which waited for: 2 -> 1; matrix products, arithmetic and copies ran while one was open for 0% -> 0% of each run, Pallas kernels for 0% -> 0%
where the time goes in v3:
time: 51.2 us; the launch traced here: 51.6 us
  blocking collectives  35.7 us (70%)
  Pallas kernels  13.4 us (26%)
  waiting for transfers between devices  1.62 us (3%)
  between operations  0.7 us (1%)
    all_to_all x1, blocking collectives, shards(): lax.all_to_all(send.reshape(half_count, block, LANES), 'ep', split_axis=0...  21.5 us
    all_to_all x1, blocking collectives, shards(): lax.all_to_all(outputs.reshape(half_count, block, LANES), 'ep', split_axi...  14.2 us
    pallas_call x1, Pallas kernels, run_mixer(): pl.pallas_call(mixer(n_seq, n_pos, width, lat, expert_count, slot_count),...  11.5 us
    ppermute x2, waiting for transfers between devices, partner(): return lax.ppermute(value, axis, pairs)  1.62 us
  transfers between devices with their start and end apart: 2, of which 1 were waited for; matrix products, arithmetic and copies ran while one was open for 0% of the time, Pallas kernels for 0%

profile of v3, /device:TPU:0, one launch (start us, length us, event | category | flops | bytes accessed | tf_op | source)
XLA Modules:
  0.0 51.6 jit_solution(3709895735821741421)
XLA Ops:
  0.6 11.5 %mixer.1 = (f32[12,2048]{1,0:T(8,128)}, bf16[12,512]{1,0:T(8,128)(2,1)}, bf16[12,64]{1,0:T(8,128)(2,1)}, bf16[16,2,40,128]{3,2,1,0:T(8,128)(2,1)S(1)}, bf16[2,12...) custom-call(s32[1]{0:T(128)} %bitcast.side_ref, ...), custom_call_target="tpu_custom_call" | custom-call | tf_op jit(solution)/shard_map/mixer/pallas_call | solution.py:448
  12.1 0.1 collective-permute-start
  12.2 21.5 %all_to_all.10 = bf16[32,40,128]{2,1,0:T(8,128)(2,1)S(1)} all-to-all(bf16[32,40,128]{2,1,0:T(8,128)(2,1)S(1)} %bitcast.19), channel_id=1, replica_groups=mesh['ep'=32] {'ep'}, dimensions={0} | all-to-all | bytes 655360 | tf_op jit(solution)/shard_map/all_to_all | solution.py:643
  33.7 0.0 collective-permute-done.other_ref
  33.7 0.5 %expert_inner.1 = (f32[160,1024]{1,0:T(8,128)S(1)}, bf16[160,1024]{1,0:T(8,128)(2,1)S(1)}) custom-call(bf16[1280,128]{1,0:T(8,128)(2,1)S(1)} %bitcast.17, bf16[1024,256]{1,0:T(8,128)(2,1)S(1)} %get-tuple-element.17.gate_ref, bf16[1024,256]{1,0:T(8,128)(2,1)S(1)} %get-tuple-element.18.up_ref, bf16[3072,256]{1,0:T(8,128)(2,1)S(1)} %collective-permute-done.other_ref), custom_call_target="tpu_custom_call" | custom-call | tf_op jit(solution)/shard_map/expert_inner/pallas_call | solution.py:524
  34.2 0.0 copy-start
  34.3 0.0 copy-start.1
  34.3 0.1 collective-permute-start.1
  34.3 1.6 %collective-permute-done.1.given_ref = bf16[160,1024]{1,0:T(8,128)(2,1)S(1)} collective-permute-done((bf16[160,1024]{1,0:T(8,128)(2,1)S(1)}, bf16[160,1024]{1,0:T(8,128)(2,1)S(1)}, u32[]{:S(2)}, u32[]{:S(2)}) %collective-permute-start.1) | collective-permute-done | bytes 327712 | tf_op jit(solution)/shard_map/ppermute | solution.py:39
  36.0 0.4 expert_outer.1
  36.4 14.2 %all_to_all.11 = bf16[32,40,128]{2,1,0:T(8,128)(2,1)S(1)} all-to-all(bf16[32,40,128]{2,1,0:T(8,128)(2,1)S(1)} %bitcast.18), channel_id=1, replica_groups=mesh['ep'=32] {'ep'}, dimensions={0} | all-to-all | bytes 655360 | tf_op jit(solution)/shard_map/all_to_all | solution.py:648
  50.6 0.0 copy-done
  50.6 0.0 copy-done.1
  50.6 1.0 %combine.1 = f32[12,2048]{1,0:T(8,128)} custom-call(f32[12,2048]{1,0:T(8,128)S(1)} %copy-done.1, bf16[2,128,640]{2,1,0:T(8,128)(2,1)S(1)} %copy-done, bf16[16,2,40,128]{3,2,1,0:T(8,128)(2,1)S(1)} %bitcast.16), custom_call_target="tpu_custom_call" | custom-call | tf_op jit(solution)/shard_map/combine/pallas_call | solution.py:594
Async XLA Ops:
  12.1 21.6 %collective-permute-start = (bf16[3072,256]{1,0:T(8,128)(2,1)S(1)}, bf16[3072,256]{1,0:T(8,128)(2,1)S(1)}, u32[]{:S(2)}, u32[]{:S(2)}) collective-permute-start(bf16[3072,256]{1,0:T(8,128)(2,1)S(1)} %get-tuple-element.19), channel_id=1, source_target_pairs={{0,1},{1,0},{2,3},{3,2},{4,5},{5,4},{6,7},{7,6},{8,9},{9,8},{10,11... | collective-permute-start | bytes 4718600 | tf_op jit(solution)/shard_map/ppermute | solution.py:39
  34.2 16.3 %copy-start = (bf16[2,128,640]{2,1,0:T(8,128)(2,1)S(1)}, bf16[2,128,640]{2,1,0:T(8,128)(2,1)}, u32[]{:S(2)}) copy-start(bf16[2,128,640]{2,1,0:T(8,128)(2,1)} %get-tuple-element.15.combine_ref) | copy-start | bytes 983044
  34.3 16.3 %copy-start.1 = (f32[12,2048]{1,0:T(8,128)S(1)}, f32[12,2048]{1,0:T(8,128)}, u32[]{:S(2)}) copy-start(f32[12,2048]{1,0:T(8,128)} %get-tuple-element.14.mixed_ref) | copy-start | bytes 294916
  34.3 1.7 %collective-permute-start.1 = (bf16[160,1024]{1,0:T(8,128)(2,1)S(1)}, bf16[160,1024]{1,0:T(8,128)(2,1)S(1)}, u32[]{:S(2)}, u32[]{:S(2)}) collective-permute-start(bf16[160,1024]{1,0:T(8,128)(2,1)S(1)} %get-tuple-element.21), channel_id=1, source_target_pairs={{0,1},{1,0},{2,3},{3,2},{4,5},{5,4},{6,7},{7,6},{8,9},{9,8},{10,11... | collective-permute-start | bytes 983048 | tf_op jit(solution)/shard_map/ppermute | solution.py:39

commit v4 on v3

--- a/solution.py
+++ b/solution.py
@@ -15,8 +15,8 @@
 SEQ_DEV = 12
 LANES = 128
 ROWS = 16
-SEQ_STEP = 4
-GROUPS_AHEAD = 3
+SEQ_STEP = 3
+GROUPS_AHEAD = 4
 BLOCK_POS = 256
 
 EPS = 1e-06
@@ -177,32 +177,32 @@
         group_count = n_seq // SEQ_STEP
         most_blocks = pl.cdiv(n_pos, BLOCK_POS)
 
-        def latent_copy(group, j, block):
-            slot = group * SEQ_STEP + j
-            rows = pl.ds(block * BLOCK_POS, min(BLOCK_POS, n_pos - block * BLOCK_POS))
-            return pltpu.make_async_copy(
-                latent_hbm.at[order_s[slot], rows, :],
-                latent.at[slot, rows, :],
-                c_sem.at[slot, block],
-            )
-
-        def rope_copy(group, j):
-            slot = group * SEQ_STEP + j
-            return pltpu.make_async_copy(rope_hbm.at[order_s[slot]], rope.at[slot], r_sem.at[slot])
-
-        def each_copy(group, act):
+        def for_blocks(group, act):
             for block in range(most_blocks):
 
-                @pl.when(blocks_s[group] > block)
-                def _(block=block):
-                    for j in range(SEQ_STEP):
-                        act(latent_copy(group, j, block))
-
-            for j in range(SEQ_STEP):
-                act(rope_copy(group, j))
+                @pl.when(blocks_s[group] == block + 1)
+                def _(count=min(n_pos, (block + 1) * BLOCK_POS)):
+                    act(group, count)
+
+        def latent_copies(group, count):
+            slots = [group * SEQ_STEP + j for j in range(SEQ_STEP)]
+            return [
+                pltpu.make_async_copy(
+                    latent_hbm.at[order_s[slot], :count, :],
+                    latent.at[slot, :count, :],
+                    c_sem.at[slot],
+                )
+                for slot in slots
+            ]
+
+        def start_all(group, count):
+            for copy in latent_copies(group, count):
+                copy.start()
 
         def cache_start(group):
-            each_copy(group, lambda copy: copy.start())
+            for_blocks(group, start_all)
+
+        rope_copy = pltpu.make_async_copy(rope_hbm, rope, r_sem.at[0])
 
         weight_copy(0).start()
         weight_copy(1).start()
@@ -267,6 +267,7 @@
         tokens = tokens_ref[...].astype(F32)
         normed = norm_gain(tokens, attn_gain_ref[...]).astype(BF16)
         weight_copy(0).wait()
+        rope_copy.start()
         cache_start(0)
         q_low = norm_gain(mm(normed, qdown[...]), q_gain_ref[...]).astype(BF16)
         weight_copy(1).wait()
@@ -323,21 +324,16 @@
                 turned = both if side == 0 else pltpu.roll(both, ROPE_DIM, 1)
                 q_rope_s[:, head, :] = turned
 
-        def for_blocks(group, act):
-            for block in range(most_blocks):
-
-                @pl.when(blocks_s[group] == block + 1)
-                def _(count=min(n_pos, (block + 1) * BLOCK_POS)):
-                    act(group, count)
-
         def score(group, count):
+            for copy in latent_copies(group, count):
+                copy.wait()
             for j in range(SEQ_STEP):
                 slot = group * SEQ_STEP + j
                 t = order_s[slot]
                 q_lat = q_lat_s[t].astype(BF16)
                 q_rope = q_rope_s[t].astype(BF16)
                 score_s[slot, :, :count] = mm_t(q_lat, latent[slot, :count, :]) + mm(
-                    q_rope[:, :ROPE_DIM], rope[slot, :, :count]
+                    q_rope[:, :ROPE_DIM], rope[t, :, :count]
                 )
 
         def weigh(group, count):
@@ -350,8 +346,6 @@
             def _():
                 cache_start(group + GROUPS_AHEAD)
 
-            each_copy(group, lambda copy: copy.wait())
-
             @pl.when(group == 0)
             def _():
                 weight_copy(5).start()
@@ -369,6 +363,7 @@
             for_blocks(group, weigh)
             return carry
 
+        rope_copy.wait()
         lax.fori_loop(0, group_count, score_step, 0)
 
         position = lax.broadcasted_iota(jnp.int32, (HEADS, n_pos), 1)
@@ -482,8 +477,8 @@
             pltpu.VMEM((n_seq, lat), F32),
             pltpu.VMEM((n_seq, LANES), F32),
             pltpu.SemaphoreType.DMA((12 + half // hidden,)),
-            pltpu.SemaphoreType.DMA((n_seq, pl.cdiv(n_pos, BLOCK_POS))),
             pltpu.SemaphoreType.DMA((n_seq,)),
+            pltpu.SemaphoreType.DMA((1,)),
             pltpu.SemaphoreType.DMA((len(small),)),
             pltpu.SemaphoreType.DMA((2,)),
         ],
@@ -578,9 +573,11 @@
 
     def body(mixed_ref, combine_ref, rows_ref, out_ref):
         expert_count, _, rows_per, _ = rows_ref.shape
+        combine = combine_ref[...].reshape(2 * LANES, expert_count * rows_per)
         for side in range(2):
             rows = rows_ref[:, side].reshape(expert_count * rows_per, LANES)
-            total = mm(combine_ref[0], rows) + mm(combine_ref[1], rows)
+            both = mm(combine, rows)
+            total = both[:LANES] + both[LANES:]
             for r in range(chunks):
                 col = slice(side * half + r * LANES, side * half + (r + 1) * LANES)
                 out_ref[:, col] = mixed_ref[:, col] + total[r * ROWS : r * ROWS + n_seq, :]

time: 51.2 us -> 49.9 us (0.975); the launches traced: 51.6 us -> 49.1 us
  blocking collectives: 35.7 us -> 32.7 us
    all_to_all x1, blocking collectives: 21.5 us -> 18.5 us  [shards(): lax.all_to_all(send.reshape(half_count, block, LANES), 'ep', split_axis=0...]
where the time goes in v4:
time: 49.9 us; the launch traced here: 49.1 us
  blocking collectives  32.7 us (66%)
  Pallas kernels  13.9 us (28%)
  waiting for transfers between devices  1.62 us (3%)
  between operations  0.7 us (1%)
    all_to_all x1, blocking collectives, shards(): lax.all_to_all(send.reshape(half_count, block, LANES), 'ep', split_axis=0...  18.5 us
    all_to_all x1, blocking collectives, shards(): lax.all_to_all(outputs.reshape(half_count, block, LANES), 'ep', split_axi...  14.2 us
    pallas_call x1, Pallas kernels, run_mixer(): pl.pallas_call(mixer(n_seq, n_pos, width, lat, expert_count, slot_count),...  12 us
    ppermute x2, waiting for transfers between devices, partner(): return lax.ppermute(value, axis, pairs)  1.62 us
  transfers between devices with their start and end apart: 2, of which 1 were waited for; matrix products, arithmetic and copies ran while one was open for 0% of the time, Pallas kernels for 0%

profile of v4, /device:TPU:0, one launch (start us, length us, event | category | flops | bytes accessed | tf_op | source)
XLA Modules:
  0.0 49.1 jit_solution(11365180290734118371)
XLA Ops:
  0.6 12.0 %mixer.1 = (f32[12,2048]{1,0:T(8,128)}, bf16[12,512]{1,0:T(8,128)(2,1)}, bf16[12,64]{1,0:T(8,128)(2,1)}, bf16[16,2,40,128]{3,2,1,0:T(8,128)(2,1)S(1)}, bf16[2,12...) custom-call(s32[1]{0:T(128)} %bitcast.side_ref, ...), custom_call_target="tpu_custom_call" | custom-call | tf_op jit(solution)/shard_map/mixer/pallas_call | solution.py:443
  12.6 0.1 collective-permute-start
  12.7 18.5 %all_to_all.10 = bf16[32,40,128]{2,1,0:T(8,128)(2,1)S(1)} all-to-all(bf16[32,40,128]{2,1,0:T(8,128)(2,1)S(1)} %bitcast.19), channel_id=1, replica_groups=mesh['ep'=32] {'ep'}, dimensions={0} | all-to-all | bytes 655360 | tf_op jit(solution)/shard_map/all_to_all | solution.py:640
  31.2 0.0 collective-permute-done.other_ref
  31.2 0.5 %expert_inner.1 = (f32[160,1024]{1,0:T(8,128)S(1)}, bf16[160,1024]{1,0:T(8,128)(2,1)S(1)}) custom-call(bf16[1280,128]{1,0:T(8,128)(2,1)S(1)} %bitcast.17, bf16[1024,256]{1,0:T(8,128)(2,1)S(1)} %get-tuple-element.17.gate_ref, bf16[1024,256]{1,0:T(8,128)(2,1)S(1)} %get-tuple-element.18.up_ref, bf16[3072,256]{1,0:T(8,128)(2,1)S(1)} %collective-permute-done.other_ref), custom_call_target="tpu_custom_call" | custom-call | tf_op jit(solution)/shard_map/expert_inner/pallas_call | solution.py:519
  31.7 0.0 copy-start
  31.7 0.0 copy-start.1
  31.8 0.1 collective-permute-start.1
  31.8 1.6 %collective-permute-done.1.given_ref = bf16[160,1024]{1,0:T(8,128)(2,1)S(1)} collective-permute-done((bf16[160,1024]{1,0:T(8,128)(2,1)S(1)}, bf16[160,1024]{1,0:T(8,128)(2,1)S(1)}, u32[]{:S(2)}, u32[]{:S(2)}) %collective-permute-start.1) | collective-permute-done | bytes 327712 | tf_op jit(solution)/shard_map/ppermute | solution.py:39
  33.5 0.4 expert_outer.1
  33.9 14.2 %all_to_all.11 = bf16[32,40,128]{2,1,0:T(8,128)(2,1)S(1)} all-to-all(bf16[32,40,128]{2,1,0:T(8,128)(2,1)S(1)} %bitcast.18), channel_id=1, replica_groups=mesh['ep'=32] {'ep'}, dimensions={0} | all-to-all | bytes 655360 | tf_op jit(solution)/shard_map/all_to_all | solution.py:645
  48.1 0.0 copy-done
  48.1 0.0 copy-done.1
  48.1 1.0 %combine.1 = f32[12,2048]{1,0:T(8,128)} custom-call(f32[12,2048]{1,0:T(8,128)S(1)} %copy-done.1, bf16[2,128,640]{2,1,0:T(8,128)(2,1)S(1)} %copy-done, bf16[16,2,40,128]{3,2,1,0:T(8,128)(2,1)S(1)} %bitcast.16), custom_call_target="tpu_custom_call" | custom-call | tf_op jit(solution)/shard_map/combine/pallas_call | solution.py:591
Async XLA Ops:
  12.6 18.6 %collective-permute-start = (bf16[3072,256]{1,0:T(8,128)(2,1)S(1)}, bf16[3072,256]{1,0:T(8,128)(2,1)S(1)}, u32[]{:S(2)}, u32[]{:S(2)}) collective-permute-start(bf16[3072,256]{1,0:T(8,128)(2,1)S(1)} %get-tuple-element.19), channel_id=1, source_target_pairs={{0,1},{1,0},{2,3},{3,2},{4,5},{5,4},{6,7},{7,6},{8,9},{9,8},{10,11... | collective-permute-start | bytes 4718600 | tf_op jit(solution)/shard_map/ppermute | solution.py:39
  31.7 16.3 %copy-start = (bf16[2,128,640]{2,1,0:T(8,128)(2,1)S(1)}, bf16[2,128,640]{2,1,0:T(8,128)(2,1)}, u32[]{:S(2)}) copy-start(bf16[2,128,640]{2,1,0:T(8,128)(2,1)} %get-tuple-element.15.combine_ref) | copy-start | bytes 983044
  31.7 16.3 %copy-start.1 = (f32[12,2048]{1,0:T(8,128)S(1)}, f32[12,2048]{1,0:T(8,128)}, u32[]{:S(2)}) copy-start(f32[12,2048]{1,0:T(8,128)} %get-tuple-element.14.mixed_ref) | copy-start | bytes 294916
  31.8 1.7 %collective-permute-start.1 = (bf16[160,1024]{1,0:T(8,128)(2,1)S(1)}, bf16[160,1024]{1,0:T(8,128)(2,1)S(1)}, u32[]{:S(2)}, u32[]{:S(2)}) collective-permute-start(bf16[160,1024]{1,0:T(8,128)(2,1)S(1)} %get-tuple-element.21), channel_id=1, source_target_pairs={{0,1},{1,0},{2,3},{3,2},{4,5},{5,4},{6,7},{7,6},{8,9},{9,8},{10,11... | collective-permute-start | bytes 983048 | tf_op jit(solution)/shard_map/ppermute | solution.py:39
